TPU v7x, 32 devices: a whole 2x2x4 slice. The times are simulated.
32 devices in a mesh: fs: 8 (over z, x), tp: 4 (over y, core).
Axes of the slice: x: 2, y: 2, z: 4, core: 2. Of those that a mesh axis runs over, the one named last changes fastest.
Arguments:
- x_late: bfloat16 [3072, 2048], P(('fs', 'tp')), may hold values from -6 to 6
- x_early: bfloat16 [3072, 2048], P(('fs', 'tp')), may hold values from -6 to 6
- cotangent: bfloat16 [3072, 2048], P(('fs', 'tp')), may hold values from -6 to 6
- up_weight: bfloat16 [2048, 4096], P('fs', 'tp'), may hold values from -0.125 to 0.125
- down_weight: bfloat16 [2048, 4096], P('fs', 'tp'), may hold values from -0.09375 to 0.09375
- up_grad_sum: float32 [2048, 4096], P('fs', 'tp'), may hold values from -24 to 24
- down_grad_sum: float32 [2048, 4096], P('fs', 'tp'), may hold values from -24 to 24
Outputs:
- output: bfloat16 [3072, 2048], P(('fs', 'tp'))
- input_grad: bfloat16 [3072, 2048], P(('fs', 'tp'))
- up_grad_new: float32 [2048, 4096], P('fs', 'tp')
- down_grad_new: float32 [2048, 4096], P('fs', 'tp')
All inputs are finite; a program needn't handle non-finite values.
Results may differ from a plain program's by a relative error of at most 0.0095.
Values may be sent and summed in bfloat16 or wider, within the bound.
A program may use at most 128 MiB of HBM per device.

v0:
```python
import functools

import jax
import jax.numpy as jnp
from jax import lax
from jax.experimental import pallas as pl
from jax.experimental.pallas import tpu as pltpu
from jax.sharding import PartitionSpec as P


MESH = pl.DeviceIdType.MESH
ANY = pl.BlockSpec(memory_space=pl.ANY)
VMEM = pl.BlockSpec(memory_space=pltpu.VMEM)


def dot_last(left, right):
    return lax.dot_general(
        left, right, (((1,), (1,)), ((), ())), preferred_element_type=jnp.float32
    )


def dot_first(left, right):
    return lax.dot_general(
        left, right, (((0,), (0,)), ((), ())), preferred_element_type=jnp.float32
    )


def squared(pre_act):
    return jnp.square(jax.nn.relu(pre_act)).astype(jnp.bfloat16)


def hidden_grad(grad_act, pre_early):
    return (grad_act * 2.0 * jax.nn.relu(pre_early)).astype(jnp.bfloat16)


def flip(value, bit):
    return value + bit - 2 * bit * ((value // bit) % 2)


def remote(src, dst, send, recv, fs, tp):
    return pltpu.make_async_remote_copy(
        src_ref=src, dst_ref=dst, send_sem=send, recv_sem=recv,
        device_id={"fs": fs, "tp": tp}, device_id_type=MESH,
    )


def greet(peers):
    barrier = pltpu.get_barrier_semaphore()
    for fs, tp in peers:
        pl.semaphore_signal(barrier, inc=1, device_id={"fs": fs, "tp": tp}, device_id_type=MESH)
    pl.semaphore_wait(barrier, len(peers))


def gather_kernel(n_fo, n_tp, *refs):
    tokens, weights = refs[0:3], refs[3:5]
    all_tokens, all_weights = refs[5:8], refs[8:10]
    local, t_send, t_recv, x_send, x_recv, z_send, z_recv = refs[10:]
    fs, tp = lax.axis_index("fs"), lax.axis_index("tp")
    fo, fi = fs // 2, fs % 2
    pair = fo * 2 + 1 - fi
    half = weights[0].shape[1] // 2
    dims = n_tp.bit_length()

    def placed(mask):
        at_fi, at_tp = (1 - fi if mask & 1 else fi), tp
        for dim in range(1, dims):
            if (mask >> dim) & 1:
                at_tp = flip(at_tp, n_tp >> dim)
        return at_fi, at_tp

    def token(a, dim, mask):
        to_fi, to_tp = placed(1 << dim)
        slot = placed(mask)
        dst = all_tokens[a].at[slot[0], slot[1]]
        sem = mask + (1 << dim)
        return remote(tokens[a] if mask == 0 else dst, dst, t_send.at[a, sem], t_recv.at[a, sem],
                      fo * 2 + to_fi, to_tp)

    def columns(w, which):
        return weights[w].at[:, pl.ds(pl.multiple_of(which * half, half), half)]

    def across(w):
        return remote(columns(w, 1 - fi), all_weights[w].at[fs], x_send.at[w], x_recv.at[w], pair, tp)

    def along(w, source, part, way):
        dst = all_weights[w].at[source * 2 + (1 - fi if part else fi)]
        return dst, z_send.at[way, w, source, part], z_recv.at[w, source, part], ((fo + 1 - 2 * way) % n_fo) * 2 + fi

    def relay(w, source, part, way):
        dst, send, recv, to = along(w, source, part, way)
        return remote(dst, dst, send, recv, to, tp)

    def begin(w, way):
        dst, send, recv, to = along(w, fo, 0, way)
        return remote(columns(w, fi), dst, send, recv, to, tp)

    def open_way(way):
        return fo < n_fo - 1 if way == 0 else fo > 0

    def take(w, part, distance):
        for way in range(2):
            source = fo - distance if way == 0 else fo + distance

            @pl.when((source >= 0) & (source < n_fo))
            def _():
                relay(w, source, part, way).wait_recv()

                @pl.when(open_way(way))
                def _():
                    relay(w, source, part, way).start()

    peers = []
    for dim in range(dims):
        to_fi, to_tp = placed(1 << dim)
        peers.append((fo * 2 + to_fi, to_tp))
    for step in (1, n_fo - 1):
        peers.append((((fo + step) % n_fo) * 2 + fi, tp))
    greet(peers)

    for way in range(2):
        @pl.when(open_way(way))
        def _():
            for w in range(2):
                begin(w, way).start()
    for a in range(3):
        token(a, 0, 0).start()
        if a < 2:
            across(a).start()
    for a in range(3):
        for dim in range(1, dims):
            token(a, dim, 0).start()
    own = [pltpu.make_async_copy(tokens[a], all_tokens[a].at[fi, tp], local.at[a]) for a in range(3)]
    own += [pltpu.make_async_copy(columns(w, fi), all_weights[w].at[fs], local.at[3 + w]) for w in range(2)]
    for copy in own:
        copy.start()

    def passed(a, dim, mask):
        token(a, dim, mask).wait_recv()
        for later in range(dim + 1, dims):
            token(a, later, mask + (1 << dim)).start()

    def crossed(w):
        across(w).wait_recv()
        for way in range(2):
            @pl.when(open_way(way))
            def _():
                relay(w, fo, 1, way).start()

    take(0, 0, 1)
    take(1, 0, 1)
    passed(0, 0, 0)
    crossed(0)
    for distance in range(2, n_fo):
        take(0, 0, distance)
        take(1, 0, distance)
        if distance == 2:
            passed(1, 0, 0)
            crossed(1)
            take(0, 1, 1)
            passed(2, 0, 0)
    take(1, 1, 1)
    for distance in range(2, n_fo - 1):
        take(0, 1, distance)
        take(1, 1, distance)
    for dim in range(1, dims):
        for mask in range(1 << dim):
            for a in range(3):
                passed(a, dim, mask)
    for w in range(2):
        take(w, 1, n_fo - 1)
        across(w).wait_send()
        for way in range(2):
            @pl.when(open_way(way))
            def _():
                begin(w, way).wait_send()
                relay(w, fo, 1, way).wait_send()
                for distance in range(1, n_fo):
                    source = fo - distance if way == 0 else fo + distance

                    @pl.when((source >= 0) & (source < n_fo))
                    def _():
                        for part in range(2):
                            relay(w, source, part, way).wait_send()
    for dim in range(dims):
        for a in range(3):
            for mask in range(1 << dim):
                token(a, dim, mask).wait_send()
    for copy in own:
        copy.wait()


def gather(n_fo, n_tp, tokens, weights):
    rows, width = tokens[0].shape
    w_rows, cols = weights[0].shape
    masks = 2 * n_tp
    dma = pltpu.SemaphoreType.DMA
    return pl.pallas_call(
        functools.partial(gather_kernel, n_fo, n_tp),
        out_shape=[jax.ShapeDtypeStruct((2, n_tp, rows, width), jnp.bfloat16)] * 3
        + [jax.ShapeDtypeStruct((2 * n_fo, w_rows, cols // 2), jnp.bfloat16)] * 2,
        in_specs=[VMEM] * 5,
        out_specs=[ANY] * 5,
        scratch_shapes=[
            dma((5,)), dma((3, masks)), dma((3, masks)), dma((2,)), dma((2,)),
            dma((2, 2, n_fo, 2)), dma((2, n_fo, 2)),
        ],
        compiler_params=pltpu.CompilerParams(collective_id=0, has_side_effects=True),
        name="gather",
    )(*tokens, *weights)


def reduce_kernel(n_fo, n_tp, *refs):
    partial, grads = refs[0:2], refs[2:4]
    summed, mine, other = refs[4:6], refs[6:8], refs[8:10]
    (landed, pair_sum, arrived, g_in, staged,
     c_send, c_recv, t_send, t_recv, z_send, z_recv, x_send, x_recv) = refs[10:]
    fs, tp = lax.axis_index("fs"), lax.axis_index("tp")
    fo, fi = fs // 2, fs % 2
    pair = fo * 2 + 1 - fi
    n_y = n_tp // 2
    y, core = tp // 2, tp % 2
    others = [(dx, dy) for dy in range(n_y) for dx in range(2) if (dx, dy) != (0, 0)]

    def spot(dx, dy):
        return (1 - fi if dx else fi), (y + dy) % n_y

    def near(a):
        return remote(partial[a].at[:, :, 1 - core], landed.at[a], c_send.at[a], c_recv.at[a],
                      fs, y * 2 + 1 - core)

    def far(a, k):
        at_fi, at_y = spot(*others[k])
        return remote(pair_sum.at[a, at_fi, at_y], arrived.at[a, k], t_send.at[a, k], t_recv.at[a, k],
                      fo * 2 + at_fi, at_y * 2 + core)

    def along(w, block, way, src):
        return remote(src, g_in.at[way, w, block], z_send.at[way, w, block], z_recv.at[way, w, block],
                      ((fo + 1 - 2 * way) % n_fo) * 2 + fi, tp)

    def onward(way, distance, action):
        block = fo + distance if way == 0 else fo - distance
        first = fo == 0 if way == 0 else fo == n_fo - 1
        inside = (block >= 0) & (block < n_fo)
        for w in range(2):
            action(w, block, first, inside)

    def across(w):
        return remote(staged.at[w], other[w], x_send.at[w], x_recv.at[w], pair, tp)

    peers = [(fs, y * 2 + 1 - core)]
    for dx, dy in others:
        at_fi, at_y = spot(dx, dy)
        peers.append((fo * 2 + at_fi, at_y * 2 + core))
    for step in (1, n_fo - 1):
        peers.append((((fo + step) % n_fo) * 2 + fi, tp))
    greet(peers)

    for a in range(2):
        near(a).start()
    for way in range(2):
        def launch(w, block, first, inside):
            @pl.when(first & inside)
            def _():
                along(w, block, way, grads[w].at[block]).start()

        for distance in range(n_fo - 1, 0, -1):
            onward(way, distance, launch)

    def joined(a, at_fi, at_y):
        return (partial[a][at_fi, at_y, core].astype(jnp.float32)
                + landed[a, at_fi, at_y].astype(jnp.float32))

    for a in range(2):
        near(a).wait_recv()
        for k in range(len(others)):
            at_fi, at_y = spot(*others[k])
            pair_sum[a, at_fi, at_y] = joined(a, at_fi, at_y).astype(jnp.bfloat16)
            far(a, k).start()

    for distance in range(n_fo - 2, 0, -1):
        for way in range(2):
            def carry(w, block, first, inside):
                @pl.when(jnp.logical_not(first) & inside)
                def _():
                    held = g_in.at[way, w, block]
                    along(w, block, way, held).wait_recv()
                    for part in range(2):
                        g_in[way, w, block, part] = (
                            grads[w][block, part].astype(jnp.float32)
                            + g_in[way, w, block, part].astype(jnp.float32)
                        ).astype(jnp.bfloat16)
                    along(w, block, way, held).start()

            onward(way, distance, carry)

    def owned(w, which):
        return (grads[w][fo, which].astype(jnp.float32)
                + g_in[0, w, fo, which].astype(jnp.float32)
                + g_in[1, w, fo, which].astype(jnp.float32))

    for w in range(2):
        for way in range(2):
            first = fo == 0 if way == 0 else fo == n_fo - 1

            @pl.when(first)
            def _():
                g_in[way, w, fo] = jnp.zeros(g_in.shape[3:], g_in.dtype)

            @pl.when(jnp.logical_not(first))
            def _():
                along(w, fo, way, g_in.at[way, w, fo]).wait_recv()
        staged[w] = owned(w, 1 - fi).astype(jnp.bfloat16)
        across(w).start()
        mine[w][...] = owned(w, fi)
    for a in range(2):
        total = joined(a, fi, y)
        for k in range(len(others)):
            far(a, k).wait_recv()
            total += arrived[a, k].astype(jnp.float32)
        summed[a][...] = total.astype(jnp.bfloat16)
    for w in range(2):
        across(w).wait()
    for way in range(2):
        def finish(w, block, first, inside):
            @pl.when(inside)
            def _():
                along(w, block, way, grads[w].at[block]).wait_send()

        for distance in range(n_fo - 1, 0, -1):
            onward(way, distance, finish)
    for a in range(2):
        near(a).wait_send()
        for k in range(len(others)):
            far(a, k).wait_send()


def reduce(n_fo, n_tp, partial, grads):
    rows, width = partial[0].shape[-2:]
    w_rows, half = grads[0].shape[-2:]
    n_y = n_tp // 2
    others = 2 * n_y - 1
    dma = pltpu.SemaphoreType.DMA
    bf16, f32 = jnp.bfloat16, jnp.float32
    return pl.pallas_call(
        functools.partial(reduce_kernel, n_fo, n_tp),
        out_shape=[jax.ShapeDtypeStruct((rows, width), bf16)] * 2
        + [jax.ShapeDtypeStruct((w_rows, half), f32)] * 2
        + [jax.ShapeDtypeStruct((w_rows, half), bf16)] * 2,
        in_specs=[VMEM] * 4,
        out_specs=[VMEM] * 6,
        scratch_shapes=[
            pltpu.VMEM((2, 2, n_y, rows, width), bf16),
            pltpu.VMEM((2, 2, n_y, rows, width), bf16),
            pltpu.VMEM((2, others, rows, width), bf16),
            pltpu.VMEM((2, 2, n_fo, 2, w_rows, half), bf16),
            pltpu.VMEM((2, w_rows, half), bf16),
            dma((2,)), dma((2,)), dma((2, others)), dma((2, others)),
            dma((2, 2, n_fo)), dma((2, 2, n_fo)), dma((2,)), dma((2,)),
        ],
        compiler_params=pltpu.CompilerParams(collective_id=1, has_side_effects=True),
        name="reduce",
    )(*partial, *grads)


def on_device(n_fo, n_tp, x_late, x_early, cotangent, up_weight, down_weight, up_grad_sum, down_grad_sum):
    rows, width = x_late.shape
    w_rows, cols = up_weight.shape
    half = cols // 2
    late, early, cot, up, down = gather(n_fo, n_tp, (x_late, x_early, cotangent), (up_weight, down_weight))
    late, early, cot = (a.reshape(-1, width) for a in (late, early, cot))
    up, down = (a.reshape(-1, half) for a in (up, down))
    pre_late = jnp.dot(late, up, preferred_element_type=jnp.float32)
    pre_early = jnp.dot(early, up, preferred_element_type=jnp.float32)
    act_late = squared(pre_late)
    grad_act = jnp.dot(cot, down, preferred_element_type=jnp.float32)
    act_early = squared(pre_early)
    grad_pre = hidden_grad(grad_act, pre_early)
    partial = [
        value.astype(jnp.bfloat16).reshape(2, n_tp // 2, 2, rows, width)
        for value in (dot_last(act_late, down), dot_last(grad_pre, up))
    ]
    grads = [
        value.astype(jnp.bfloat16).reshape(n_fo, 2, w_rows, half)
        for value in (dot_first(early, grad_pre), dot_first(cot, act_early))
    ]
    output, input_grad, up_mine, down_mine, up_other, down_other = reduce(n_fo, n_tp, partial, grads)
    low = lax.axis_index("fs") % 2 == 0

    def added(total, mine, other):
        other = other.astype(jnp.float32)
        return total + jnp.concatenate([jnp.where(low, mine, other), jnp.where(low, other, mine)], axis=1)

    return (output, input_grad, added(up_grad_sum, up_mine, up_other), added(down_grad_sum, down_mine, down_other))


def solution(mesh):
    rows, both = P(("fs", "tp"), None), P("fs", "tp")
    return jax.shard_map(
        functools.partial(on_device, mesh.shape["fs"] // 2, mesh.shape["tp"]),
        mesh=mesh,
        in_specs=(rows, rows, rows, both, both, both, both),
        out_specs=(rows, rows, both, both),
        check_vma=False,
    )
```

profile of v0, /device:TPU:0, one launch (start us, length us, event | category | flops | bytes accessed | tf_op | source)
XLA Modules:
  0.0 187.9 jit_solution(1494501199412738440)
XLA Ops:
  0.6 75.1 %gather.1 = (bf16[2,4,96,2048]{3,2,1,0:T(8,128)(2,1)}, bf16[2,4,96,2048]{3,2,1,0:T(8,128)(2,1)}, bf16[2,4,96,2048]{3,2,1,0:T(8,128)(2,1)}, bf16[8,256,512]{2,1,0:T(8,128)(2,1)}, bf16[8,256,512]{2,1,0:T(8,128)(2,1)}) custom-call(bf16[96,2048]{1,0:T(8,128)(2,1)} %refs_0_.1, bf16[96,2048]{1,0:T(8,128)(2,1)} %refs_1_.1, bf16[96,2048]{1,0:T(8,128)(2,1)} %refs_2_.1, ...), custom_call_target="tpu_custom_call" | custom-call | tf_op jit(solution)/shard_map/gather/pallas_call | solution.py:197
  75.8 0.0 copy-start.4
  75.8 8.4 %convolution_convert_fusion.1 = bf16[768,2048]{1,0:T(8,128)(2,1)} fusion(bf16[2048,512]{1,0:T(8,128)(2,1)} %bitcast.33, bf16[768,2048]{1,0:T(8,128)(2,1)} %bitcast.29, bf16[2048,512]{1,0:T(8,128)(2,1)} %bitcast.30), kind=kOutput, calls=%fused_computation.1 | convolution fusion | flops 3223977984 | bytes 10485760 | tf_op jit(solution)/shard_map/dot_general | solution.py:17
  84.1 0.0 copy-done.4
  84.1 0.0 copy-start.5
  84.1 0.0 copy-start.7
  84.1 3.5 %convolution_maximum_fusion = f32[768,512]{1,0:T(8,128)S(1)} fusion(bf16[768,2048]{1,0:T(8,128)(2,1)S(1)} %bitcast.25, bf16[2048,512]{1,0:T(8,128)(2,1)} %bitcast.31), kind=kOutput, calls=%fused_computation.7 | convolution fusion | flops 1611005952 | bytes 6815744 | tf_op jit(solution)/shard_map/dot_general | solution.py:373
  87.7 0.0 copy-done.5
  87.7 0.0 copy-done.7
  87.7 1.8 multiply_convert_fusion.1
  89.5 3.2 %convolution_convert_fusion.2 = bf16[2048,512]{1,0:T(8,128)(2,1)} fusion(bf16[768,2048]{1,0:T(8,128)(2,1)S(1)} %bitcast.28, f32[768,512]{1,0:T(8,128)S(1)} %convolution_maximum_fusion), kind=kOutput, calls=%fused_computation.2 | convolution fusion | flops 1612447744 | bytes 6815744 | tf_op jit(solution)/shard_map/dot_general | solution.py:23
  92.7 0.0 copy-start.6
  92.7 3.2 %convolution_convert_fusion.3 = bf16[2048,512]{1,0:T(8,128)(2,1)} fusion(bf16[768,2048]{1,0:T(8,128)(2,1)S(1)} %bitcast.26, bf16[768,512]{1,0:T(8,128)(2,1)S(1)} %multiply_convert_fusion.1), kind=kOutput, calls=%fused_computation.3 | convolution fusion | flops 1611661312 | bytes 6029312 | tf_op jit(solution)/shard_map/dot_general | solution.py:23
  95.9 0.0 copy-done.6
  95.9 3.5 %convolution_convert_fusion = bf16[768,2048]{1,0:T(8,128)(2,1)} fusion(bf16[768,512]{1,0:T(8,128)(2,1)S(1)} %multiply_convert_fusion.1, bf16[2048,512]{1,0:T(8,128)(2,1)S(1)} %bitcast.32), kind=kOutput, calls=%fused_computation | convolution fusion | flops 1612185600 | bytes 6029312 | tf_op jit(solution)/shard_map/dot_general | solution.py:17
  99.4 82.6 %reduce.1 = (bf16[96,2048]{1,0:T(8,128)(2,1)}, bf16[96,2048]{1,0:T(8,128)(2,1)}, f32[256,512]{1,0:T(8,128)}, f32[256,512]{1,0:T(8,128)}, bf16[256,512]{1,0:T(8,128)(2,1)}, /*index=5*/bf16[256,512]{1,0:T(8,128)(2,1)}) custom-call(bf16[2,2,2,96,2048]{4,3,2,1,0:T(8,128)(2,1)} %bitcast.21, bf16[2,2,2,96,2048]{4,3,2,1,0:T(8,128)(2,1)} %bitcast.22, ...), custom_call_target="tpu_custom_call" | custom-call | tf_op jit(solution)/shard_map/reduce/pallas_call | solution.py:344
  182.0 0.0 copy-start
  182.0 1.7 convert_select_fusion.1
  183.7 0.0 copy-start.1
  183.7 0.0 copy-done
  183.8 1.1 maximum_add_fusion.1
  184.9 0.4 copy-done.1
  185.3 0.0 copy-start.3
  185.3 0.0 copy-start.2
  185.3 1.1 maximum_add_fusion
  186.4 0.0 copy-done.3
  186.4 0.7 copy.13
  187.2 0.0 copy-done.2
  187.2 0.7 copy.14
Async XLA Ops:
  75.8 8.4 %copy-start.4 = (bf16[2,4,96,2048]{3,2,1,0:T(8,128)(2,1)S(1)}, bf16[2,4,96,2048]{3,2,1,0:T(8,128)(2,1)}, u32[]{:S(2)}) copy-start(bf16[2,4,96,2048]{3,2,1,0:T(8,128)(2,1)} %get-tuple-element.19) | copy-start | bytes 9437188
  84.1 3.5 %copy-start.5 = (bf16[2,4,96,2048]{3,2,1,0:T(8,128)(2,1)S(1)}, bf16[2,4,96,2048]{3,2,1,0:T(8,128)(2,1)}, u32[]{:S(2)}) copy-start(bf16[2,4,96,2048]{3,2,1,0:T(8,128)(2,1)} %get-tuple-element.18) | copy-start | bytes 9437188
  84.1 3.5 %copy-start.7 = (bf16[8,256,512]{2,1,0:T(8,128)(2,1)S(1)}, bf16[8,256,512]{2,1,0:T(8,128)(2,1)}, u32[]{:S(2)}) copy-start(bf16[8,256,512]{2,1,0:T(8,128)(2,1)} %get-tuple-element.17) | copy-start | bytes 6291460
  92.7 3.2 %copy-start.6 = (bf16[8,256,512]{2,1,0:T(8,128)(2,1)S(1)}, bf16[8,256,512]{2,1,0:T(8,128)(2,1)}, u32[]{:S(2)}) copy-start(bf16[8,256,512]{2,1,0:T(8,128)(2,1)} %get-tuple-element.16) | copy-start | bytes 6291460
  182.0 1.7 copy-start
  183.7 1.6 copy-start.1
  185.3 1.1 copy-start.3
  185.3 1.9 copy-start.2
where the time goes:
time: 188 us
  Pallas kernels  158 us (84%)
  matrix products  23.6 us (13%)
  other arithmetic  3.95 us (2%)
  local copies, waits for them, and re-layouts  1.94 us (1%)
    pallas_call x1, Pallas kernels, reduce(): pl.pallas_call(functools.partial(reduce_kernel, n_fo, n_tp), out_shape=[j...  82.6 us
    pallas_call x1, Pallas kernels, gather(): pl.pallas_call(functools.partial(gather_kernel, n_fo, n_tp), out_shape=[j...  75.1 us
    dot_general x2, matrix products, dot_last(): lax.dot_general(left, right, (((1,), (1,)), ((), ())), preferred_element_...  11.9 us
    dot_general x2, matrix products, dot_first(): lax.dot_general(left, right, (((0,), (0,)), ((), ())), preferred_element_...  6.42 us

commit v1 on v0

v1 whole, which is shorter than its diff:
```python
import functools

import jax
import jax.numpy as jnp
from jax import lax
from jax.experimental import pallas as pl
from jax.experimental.pallas import tpu as pltpu
from jax.sharding import PartitionSpec as P


MESH = pl.DeviceIdType.MESH
VMEM = pl.BlockSpec(memory_space=pltpu.VMEM)
EARLY, COT, LATE = 0, 1, 2
UP, DOWN = 0, 1
CHUNKS = 2


def dot(left, right, left_dim, right_dim):
    return lax.dot_general(
        left, right, (((left_dim,), (right_dim,)), ((), ())), preferred_element_type=jnp.float32
    )


def remote(src, dst, send, recv, fs, tp):
    return pltpu.make_async_remote_copy(
        src_ref=src, dst_ref=dst, send_sem=send, recv_sem=recv,
        device_id={"fs": fs, "tp": tp}, device_id_type=MESH,
    )


def layer_kernel(n_fo, n_tp, *refs):
    tokens, weights = refs[0:3], refs[3:5]
    summed, grads = refs[5:7], refs[7:9]
    (tok, wts, g_out, g_in, pre, hid, partial, landed, pair_sum, arrived, staged, other,
     local, t_send, t_recv, a_send, a_recv, zg_send, zg_recv,
     c_send, c_recv, p_send, p_recv, zr_send, zr_recv, x_send, x_recv) = refs[9:]
    fs, tp = lax.axis_index("fs"), lax.axis_index("tp")
    fo, fi = fs // 2, fs % 2
    y, core = tp // 2, tp % 2
    pair = fo * 2 + 1 - fi
    across_y = (1 - y) * 2 + core
    sibling = y * 2 + 1 - core
    rows, width = tokens[0].shape
    w_rows, cols = weights[0].shape
    half = cols // 2
    wide = half // CHUNKS
    count = 4 * rows * 2
    cut = rows // 96 * 16
    first, last = fo == 0, fo == n_fo - 1

    def side(part):
        return 1 - fi if part else fi

    def open_way(way):
        return jnp.logical_not(last) if way == 0 else jnp.logical_not(first)

    def ahead(way):
        return (fo + 1 - 2 * way) * 2 + fi

    spots = [(0, 0), (1, 0), (0, 1), (1, 1)]

    def slot(a, k, at_core):
        dx, dy = spots[k]
        return tok.at[a, (1 - fi if dx else fi), (1 - y if dy else y), at_core]

    def token(a, j):
        sems = t_send.at[a, j], t_recv.at[a, j]
        if j == 0:
            return remote(tokens[a], slot(a, 0, core), *sems, pair, tp)
        if j == 1:
            return remote(tokens[a], slot(a, 0, core), *sems, fs, across_y)
        if j == 2:
            part = slot(a, 2, core).at[pl.ds(0, cut)]
            return remote(part, part, *sems, pair, tp)
        if j == 3:
            part = slot(a, 1, core).at[pl.ds(cut, rows - cut)]
            return remote(part, part, *sems, fs, across_y)
        k = j - 4
        dst = slot(a, k, core)
        return remote(tokens[a] if k == 0 else dst, dst, *sems, fs, sibling)

    def token_in(a, j):
        sems = t_send.at[a, j], t_recv.at[a, j]
        if j < 2:
            dst = slot(a, 1 + j, core)
        elif j == 2:
            dst = slot(a, 3, core).at[pl.ds(0, cut)]
        elif j == 3:
            dst = slot(a, 3, core).at[pl.ds(cut, rows - cut)]
        else:
            dst = slot(a, j - 4, 1 - core)
        return remote(dst, dst, *sems, fs, sibling)

    def from_y(a):
        token_in(a, 1).wait_recv()
        token(a, 2).start()
        token(a, 6).start()

    def from_x(a):
        token_in(a, 0).wait_recv()
        token(a, 3).start()
        token(a, 5).start()

    def diagonal(a):
        token_in(a, 3).wait_recv()
        token_in(a, 2).wait_recv()
        token(a, 7).start()

    def from_sibling(a):
        for k in range(4):
            token_in(a, 4 + k).wait_recv()

    def columns(w, which, c):
        return weights[w].at[:, pl.ds(pl.multiple_of(which * half + c * wide, wide), wide)]

    def across(w, c):
        return remote(columns(w, 1 - fi, c), wts.at[w, c, fo, fi], a_send.at[w, c], a_recv.at[w, c], pair, tp)

    def across_in(w, c):
        dst = wts.at[w, c, fo, 1 - fi]
        return remote(dst, dst, a_send.at[w, c], a_recv.at[w, c], pair, tp)

    def along(w, c, source, part, way, src=None):
        dst = wts.at[w, c, source, side(part)]
        return remote(dst if src is None else src, dst, zg_send.at[way, w, c, source, part],
                      zg_recv.at[w, c, source, part], ahead(way), tp)

    def begin(c, way):
        for w in range(2):
            along(w, c, fo, 0, way, columns(w, fi, c)).start()

    def begin_after(c, distance):
        for way in range(2):
            @pl.when(open_way(way) & ((fo if way == 0 else n_fo - 1 - fo) == distance))
            def _():
                begin(c, way)

    def crossed(c):
        for w in range(2):
            across_in(w, c).wait_recv()
            for way in range(2):
                @pl.when(open_way(way))
                def _():
                    along(w, c, fo, 1, way).start()

    def incoming(way, distance):
        source = fo - distance if way == 0 else fo + distance
        return source, (source >= 0) & (source < n_fo)

    def forward(c, part, distance):
        for w in range(2):
            for way in range(2):
                source, inside = incoming(way, distance)

                @pl.when(inside & open_way(way))
                def _():
                    along(w, c, source, part, way).wait_recv()
                    along(w, c, source, part, way).start()

    def settle(c):
        for part in range(2):
            for distance in range(1, n_fo):
                for w in range(2):
                    for way in range(2):
                        source, inside = incoming(way, distance)

                        @pl.when(inside & jnp.logical_not(open_way(way)))
                        def _():
                            along(w, c, source, part, way).wait_recv()

    def flat(a):
        return tok[a].reshape(count, width)

    def weight(w, c):
        return wts[w, c].reshape(width, wide)

    def activate(c):
        relu = jnp.maximum(dot(flat(EARLY), weight(UP, c), 1, 0), 0.0)
        pre[...] = relu
        hid[0, c] = (relu * relu).astype(jnp.bfloat16)

    def hidden_grad(c):
        grad_act = dot(flat(COT), weight(DOWN, c), 1, 0)
        hid[1, c] = (grad_act * 2.0 * pre[...]).astype(jnp.bfloat16)

    def activate_late(c):
        relu = jnp.maximum(dot(flat(LATE), weight(UP, c), 1, 0), 0.0)
        hid[2, c] = (relu * relu).astype(jnp.bfloat16)

    n_half = n_fo // 2
    d_half = width // 2

    def weight_grad(w, c, step):
        at = jnp.where(fo < n_half, 1 - step, step)
        lanes = pl.ds(pl.multiple_of(at * d_half, d_half), d_half)
        left = tok[EARLY if w == UP else COT, :, :, :, :, lanes].reshape(count, d_half)
        value = dot(left, hid[1 if w == UP else 0, c], 0, 0)
        g_out[w, c, pl.ds(at * n_half, n_half)] = value.astype(jnp.bfloat16).reshape(n_half, 2, w_rows, wide)
        for k in range(n_half):
            for part in (1, 0):
                for way in range(2):
                    block = farthest(way, step, k)

                    @pl.when((first if way == 0 else last) & (fo != block))
                    def _():
                        grad(w, c, block, part, way, g_out.at[w, c, block, side(part)]).start()

    def token_partial(a, h, w):
        sources = max(1, 512 // (2 * w_rows))
        lanes = sources * 2 * w_rows
        for b in range(n_fo // sources):
            total = None
            for c in range(CHUNKS):
                right = wts[w, c, b * sources:(b + 1) * sources].reshape(lanes, wide)
                term = dot(hid[h, c], right, 1, 1)
                total = term if total is None else total + term
            partial[a, :, :, :, :, b * lanes:(b + 1) * lanes] = (
                total.astype(jnp.bfloat16).reshape(2, 2, 2, rows, lanes))
        near(a).start()

    def farthest(way, step, k):
        return n_fo - 1 - step * n_half - k if way == 0 else step * n_half + k

    def grad(w, c, block, part, way, src=None):
        held = g_in.at[way, w, c, block, part]
        return remote(held if src is None else src, held, zr_send.at[way, w, c, block, part],
                      zr_recv.at[way, w, c, block, part], ahead(way), tp)

    def carry(w, c, step, k):
        for part in (1, 0):
            for way in range(2):
                block = farthest(way, step, k)
                inside = (fo < block) & (fo > 0) if way == 0 else (fo > block) & (fo < n_fo - 1)

                @pl.when(inside)
                def _():
                    grad(w, c, block, part, way).wait_recv()
                    g_in[way, w, c, block, part] = (
                        g_out[w, c, block, side(part)].astype(jnp.float32)
                        + g_in[way, w, c, block, part].astype(jnp.float32)
                    ).astype(jnp.bfloat16)
                    grad(w, c, block, part, way).start()

    def carry_all(c):
        for step in range(2):
            for w in (DOWN, UP):
                for k in range(n_half):
                    carry(w, c, step, k)

    def swap(w, c):
        return remote(staged.at[w, c], other.at[w, c], x_send.at[w, c], x_recv.at[w, c], pair, tp)

    def owned(w, c, part):
        for way in range(2):
            @pl.when(first if way == 0 else last)
            def _():
                g_in[way, w, c, fo, part] = jnp.zeros(g_in.shape[5:], g_in.dtype)

            @pl.when(jnp.logical_not(first if way == 0 else last))
            def _():
                grad(w, c, fo, part, way).wait_recv()
        total = (g_out[w, c, fo, side(part)].astype(jnp.float32)
                 + g_in[0, w, c, fo, part].astype(jnp.float32)
                 + g_in[1, w, c, fo, part].astype(jnp.float32))
        if part:
            staged[w, c] = total.astype(jnp.bfloat16)
            swap(w, c).start()
        else:
            grads[w][:, pl.ds(pl.multiple_of(fi * half + c * wide, wide), wide)] = total

    def swapped(w, c):
        swap(w, c).wait_recv()
        grads[w][:, pl.ds(pl.multiple_of((1 - fi) * half + c * wide, wide), wide)] = (
            other[w, c].astype(jnp.float32))

    def spot(k):
        dx, dy = spots[k]
        return (1 - fi if dx else fi), (1 - y if dy else y)

    def near(a):
        return remote(partial.at[a, :, :, 1 - core], landed.at[a], c_send.at[a], c_recv.at[a], fs, sibling)

    def far(a, k):
        at_fi, at_y = spot(k)
        return remote(pair_sum.at[a, at_fi, at_y], arrived.at[a, k - 1], p_send.at[a, k], p_recv.at[a, k],
                      fo * 2 + at_fi, at_y * 2 + core)

    def joined(a, at_fi, at_y):
        return (partial[a, at_fi, at_y, core].astype(jnp.float32)
                + landed[a, at_fi, at_y].astype(jnp.float32))

    def spread(a):
        near(a).wait_recv()
        for k in (3, 1, 2):
            at_fi, at_y = spot(k)
            pair_sum[a, at_fi, at_y] = joined(a, at_fi, at_y).astype(jnp.bfloat16)
            far(a, k).start()

    def collect(a):
        total = joined(a, fi, y)
        for k in (1, 2, 3):
            far(a, k).wait_recv()
            total += arrived[a, k - 1].astype(jnp.float32)
        summed[a][...] = total.astype(jnp.bfloat16)

    barrier = pltpu.get_barrier_semaphore()

    def greet(to_fs, to_tp):
        pl.semaphore_signal(barrier, inc=1, device_id={"fs": to_fs, "tp": to_tp}, device_id_type=MESH)

    greet(pair, tp)
    greet(fs, across_y)
    greet(fs, sibling)
    greet(pair, across_y)
    for way in range(2):
        @pl.when(open_way(way))
        def _():
            greet(ahead(way), tp)
    pl.semaphore_wait(barrier, 4 + (fo > 0).astype(jnp.int32) + (fo < n_fo - 1).astype(jnp.int32))

    for way in range(2):
        @pl.when(open_way(way))
        def _():
            begin(0, way)
    for w in range(2):
        across(w, 0).start()
    for a in (EARLY, COT):
        token(a, 0).start()
        token(a, 1).start()
    for w in range(2):
        across(w, 1).start()
    for a in (EARLY, COT, LATE):
        token(a, 4).start()
    own = [pltpu.make_async_copy(tokens[a], slot(a, 0, core), local.at[a]) for a in range(3)]
    own += [pltpu.make_async_copy(columns(w, fi, c), wts.at[w, c, fo, fi], local.at[3 + w * CHUNKS + c])
            for w in range(2) for c in range(CHUNKS)]
    for copy in own:
        copy.start()

    inner = range(2, n_fo - 1)
    forward(0, 0, 1)
    crossed(0)
    begin_after(1, 0)
    from_y(EARLY)
    for distance in inner:
        forward(0, 0, distance)
    from_x(EARLY)
    forward(0, 1, 1)
    begin_after(1, 1)
    from_y(COT)
    for distance in inner:
        forward(0, 1, distance)
        begin_after(1, distance)
    from_x(COT)
    token(LATE, 0).start()
    token(LATE, 1).start()
    diagonal(EARLY)
    forward(1, 0, 1)
    crossed(1)
    diagonal(COT)
    for copy in own:
        copy.wait()
    from_sibling(EARLY)
    from_sibling(COT)
    settle(0)

    activate(0)
    weight_grad(DOWN, 0, 0)
    for distance in inner:
        forward(1, 0, distance)
    hidden_grad(0)
    weight_grad(UP, 0, 0)
    forward(1, 1, 1)
    weight_grad(DOWN, 0, 1)
    weight_grad(UP, 0, 1)
    from_y(LATE)
    from_x(LATE)
    for k in range(n_half):
        carry(DOWN, 0, 0, k)
        if k == 0:
            for distance in inner:
                forward(1, 1, distance)
            diagonal(LATE)
    from_sibling(LATE)
    activate_late(0)
    for k in range(n_half):
        carry(UP, 0, 0, k)
    for w in (DOWN, UP):
        for k in range(n_half):
            carry(w, 0, 1, k)

    settle(1)
    activate(1)
    weight_grad(DOWN, 1, 0)
    hidden_grad(1)
    weight_grad(UP, 1, 0)
    weight_grad(DOWN, 1, 1)
    weight_grad(UP, 1, 1)
    token_partial(1, 1, UP)
    activate_late(1)
    spread(1)
    token_partial(0, 2, DOWN)
    for k in range(n_half):
        carry(DOWN, 1, 0, k)
        if k == 0:
            spread(0)
            for w in (DOWN, UP):
                owned(w, 0, 1)
    for k in range(n_half):
        carry(UP, 1, 0, k)
    for w in (DOWN, UP):
        for k in range(n_half):
            carry(w, 1, 1, k)
    for w in (DOWN, UP):
        owned(w, 0, 0)
    for w in (DOWN, UP):
        swapped(w, 0)
    owned(DOWN, 1, 1)
    owned(DOWN, 1, 0)
    collect(1)
    owned(UP, 1, 1)
    owned(UP, 1, 0)
    collect(0)
    for w in (DOWN, UP):
        swapped(w, 1)

    for a in range(3):
        for j in range(8):
            token(a, j).wait_send()
    for w in range(2):
        for c in range(CHUNKS):
            across(w, c).wait_send()
            swap(w, c).wait_send()
            for way in range(2):
                @pl.when(open_way(way))
                def _():
                    for part in range(2):
                        along(w, c, fo, part, way).wait_send()

                for distance in range(1, n_fo):
                    source, inside = incoming(way, distance)

                    @pl.when(inside & open_way(way))
                    def _():
                        for part in range(2):
                            along(w, c, source, part, way).wait_send()

                for block in range(n_fo):
                    @pl.when(fo < block if way == 0 else fo > block)
                    def _():
                        for part in range(2):
                            grad(w, c, block, part, way).wait_send()
    for a in range(2):
        near(a).wait_send()
        for k in (1, 2, 3):
            far(a, k).wait_send()


def layer(n_fo, n_tp, tokens, weights):
    rows, width = tokens[0].shape
    w_rows, cols = weights[0].shape
    wide = cols // 2 // CHUNKS
    count = 8 * rows
    dma = pltpu.SemaphoreType.DMA
    bf16, f32 = jnp.bfloat16, jnp.float32
    return pl.pallas_call(
        functools.partial(layer_kernel, n_fo, n_tp),
        out_shape=[jax.ShapeDtypeStruct((rows, width), bf16)] * 2
        + [jax.ShapeDtypeStruct((w_rows, cols), f32)] * 2,
        in_specs=[VMEM] * 5,
        out_specs=[VMEM] * 4,
        scratch_shapes=[
            pltpu.VMEM((3, 2, 2, 2, rows, width), bf16),
            pltpu.VMEM((2, CHUNKS, n_fo, 2, w_rows, wide), bf16),
            pltpu.VMEM((2, CHUNKS, n_fo, 2, w_rows, wide), bf16),
            pltpu.VMEM((2, 2, CHUNKS, n_fo, 2, w_rows, wide), bf16),
            pltpu.VMEM((count, wide), f32),
            pltpu.VMEM((3, CHUNKS, count, wide), bf16),
            pltpu.VMEM((2, 2, 2, 2, rows, width), bf16),
            pltpu.VMEM((2, 2, 2, rows, width), bf16),
            pltpu.VMEM((2, 2, 2, rows, width), bf16),
            pltpu.VMEM((2, 3, rows, width), bf16),
            pltpu.VMEM((2, CHUNKS, w_rows, wide), bf16),
            pltpu.VMEM((2, CHUNKS, w_rows, wide), bf16),
            dma((3 + 2 * CHUNKS,)), dma((3, 8)), dma((3, 8)), dma((2, CHUNKS)), dma((2, CHUNKS)),
            dma((2, 2, CHUNKS, n_fo, 2)), dma((2, CHUNKS, n_fo, 2)),
            dma((2,)), dma((2,)), dma((2, 4)), dma((2, 4)),
            dma((2, 2, CHUNKS, n_fo, 2)), dma((2, 2, CHUNKS, n_fo, 2)),
            dma((2, CHUNKS)), dma((2, CHUNKS)),
        ],
        compiler_params=pltpu.CompilerParams(
            collective_id=0, has_side_effects=True, vmem_limit_bytes=64_000_000),
        name="layer",
    )(*tokens, *weights)


def on_device(n_fo, n_tp, x_late, x_early, cotangent, up_weight, down_weight, up_grad_sum, down_grad_sum):
    output, input_grad, up_grad, down_grad = layer(
        n_fo, n_tp, (x_early, cotangent, x_late), (up_weight, down_weight))
    return (output, input_grad, up_grad_sum + up_grad, down_grad_sum + down_grad)


def solution(mesh):
    n_fo, n_tp = mesh.shape["fs"] // 2, mesh.shape["tp"]
    assert n_tp == 4 and n_fo % 2 == 0
    rows, both = P(("fs", "tp"), None), P("fs", "tp")
    return jax.shard_map(
        functools.partial(on_device, n_fo, n_tp),
        mesh=mesh,
        in_specs=(rows, rows, rows, both, both, both, both),
        out_specs=(rows, rows, both, both),
        check_vma=False,
    )
```

time: 188 us -> 167 us (0.89)
  matrix products: 23.6 us -> 0 us
  Pallas kernels: 158 us -> 160 us
    dot_general x6 -> x0, matrix products: 23.6 us -> none  [the longest x2 11.9 us: dot_last(): lax.dot_general(left, right, (((1,), (1,)), ((), ())), preferred_element_...]
    pallas_call x2 -> x1, Pallas kernels: 158 us -> 160 us  [layer(): pl.pallas_call(functools.partial(layer_kernel, n_fo, n_tp), out_shape=[ja...]
where the time goes in v1:
time: 167 us; the launch traced here: 166 us
  Pallas kernels  160 us (96%)
  other arithmetic  3.62 us (2%)
  local copies, waits for them, and re-layouts  1.9 us (1%)
    pallas_call x1, Pallas kernels, layer(): pl.pallas_call(functools.partial(layer_kernel, n_fo, n_tp), out_shape=[ja...  160 us

profile of v1, /device:TPU:0, one launch (start us, length us, event | category | flops | bytes accessed | tf_op | source)
XLA Modules:
  0.0 166.0 jit_solution(6611408484744109822)
XLA Ops:
  0.6 0.0 copy-start
  0.6 159.8 %layer.1 = (bf16[96,2048]{1,0:T(8,128)(2,1)}, bf16[96,2048]{1,0:T(8,128)(2,1)}, f32[256,1024]{1,0:T(8,128)}, f32[256,1024]{1,0:T(8,128)}) custom-call(bf16[96,2048]{1,0:T(8,128)(2,1)} %refs_0_.1, bf16[96,2048]{1,0:T(8,128)(2,1)} %refs_1_.1, bf16[96,2048]{1,0:T(8,128)(2,1)} %refs_2_.1, bf16[256,1024]{1,0:T(8,128)(2,1)} %refs_3_.1, bf16[256,1024]{1,0:T(8,128)(2,1)} %refs_4_.1), custom_call_target="tpu_custom_call" | custom-call | tf_op jit(solution)/shard_map/layer/pallas_call | solution.py:466
  160.4 0.0 copy-done
  160.4 0.0 copy-start.1
  160.4 0.0 copy-start.2
  160.4 2.5 %add.6 = f32[256,1024]{1,0:T(8,128)} add(f32[256,1024]{1,0:T(8,128)S(1)} %copy-done, f32[256,1024]{1,0:T(8,128)} %get-tuple-element.10) | non-fusion elementwise | flops 262144 | bytes 3145728 | tf_op jit(solution)/shard_map/add | solution.py:500
  163.0 0.0 copy-done.1
  163.0 0.0 copy-done.2
  163.0 0.0 copy-start.4
  163.0 1.1 add.7
  164.1 0.0 copy-done.4
  164.1 0.0 copy-start.3
  164.1 0.7 copy.13
  164.8 0.4 copy-done.3
  165.2 0.7 copy.14
Async XLA Ops:
  0.6 159.8 %copy-start = (f32[256,1024]{1,0:T(8,128)S(1)}, f32[256,1024]{1,0:T(8,128)}, u32[]{:S(2)}) copy-start(f32[256,1024]{1,0:T(8,128)} %param.12) | copy-start | bytes 3145732
  160.4 2.5 %copy-start.1 = (f32[256,1024]{1,0:T(8,128)S(1)}, f32[256,1024]{1,0:T(8,128)}, u32[]{:S(2)}) copy-start(f32[256,1024]{1,0:T(8,128)} %param.13) | copy-start | bytes 3145732
  160.4 2.5 %copy-start.2 = (f32[256,1024]{1,0:T(8,128)S(1)}, f32[256,1024]{1,0:T(8,128)}, u32[]{:S(2)}) copy-start(f32[256,1024]{1,0:T(8,128)} %get-tuple-element.11) | copy-start | bytes 3145732
  163.0 1.1 copy-start.4
  164.1 1.1 copy-start.3

commit v2 on v1

--- a/solution.py
+++ b/solution.py
@@ -13,6 +13,7 @@
 EARLY, COT, LATE = 0, 1, 2
 UP, DOWN = 0, 1
 CHUNKS = 2
+SKEW = 2
 
 
 def dot(left, right, left_dim, right_dim):
@@ -46,6 +47,7 @@
     wide = half // CHUNKS
     count = 4 * rows * 2
     cut = rows // 96 * 16
+    fold = rows // 96 * 32
     first, last = fo == 0, fo == n_fo - 1
 
     def side(part):
@@ -125,48 +127,47 @@
         return remote(dst if src is None else src, dst, zg_send.at[way, w, c, source, part],
                       zg_recv.at[w, c, source, part], ahead(way), tp)
 
-    def begin(c, way):
-        for w in range(2):
-            along(w, c, fo, 0, way, columns(w, fi, c)).start()
-
-    def begin_after(c, distance):
+    def begin(w, c, distance=None):
         for way in range(2):
-            @pl.when(open_way(way) & ((fo if way == 0 else n_fo - 1 - fo) == distance))
+            behind = fo if way == 0 else n_fo - 1 - fo
+
+            @pl.when(open_way(way) if distance is None else open_way(way) & (behind == distance))
             def _():
-                begin(c, way)
-
-    def crossed(c):
-        for w in range(2):
-            across_in(w, c).wait_recv()
-            for way in range(2):
-                @pl.when(open_way(way))
-                def _():
-                    along(w, c, fo, 1, way).start()
+                along(w, c, fo, 0, way, columns(w, fi, c)).start()
+
+    def crossed(w, c):
+        across_in(w, c).wait_recv()
+        for way in range(2):
+            @pl.when(open_way(way))
+            def _():
+                along(w, c, fo, 1, way).start()
 
     def incoming(way, distance):
         source = fo - distance if way == 0 else fo + distance
         return source, (source >= 0) & (source < n_fo)
 
-    def forward(c, part, distance):
-        for w in range(2):
-            for way in range(2):
-                source, inside = incoming(way, distance)
-
-                @pl.when(inside & open_way(way))
-                def _():
-                    along(w, c, source, part, way).wait_recv()
-                    along(w, c, source, part, way).start()
-
-    def settle(c):
+    def forward(w, c, part, distance):
+        for way in range(2):
+            source, inside = incoming(way, distance)
+
+            @pl.when(inside & open_way(way))
+            def _():
+                along(w, c, source, part, way).wait_recv()
+                along(w, c, source, part, way).start()
+
+    def forward_far(w, c, part):
+        for distance in range(2, n_fo - 1):
+            forward(w, c, part, distance)
+
+    def settle(w, c):
         for part in range(2):
             for distance in range(1, n_fo):
-                for w in range(2):
-                    for way in range(2):
-                        source, inside = incoming(way, distance)
-
-                        @pl.when(inside & jnp.logical_not(open_way(way)))
-                        def _():
-                            along(w, c, source, part, way).wait_recv()
+                for way in range(2):
+                    source, inside = incoming(way, distance)
+
+                    @pl.when(inside & jnp.logical_not(open_way(way)))
+                    def _():
+                        along(w, c, source, part, way).wait_recv()
 
     def flat(a):
         return tok[a].reshape(count, width)
@@ -199,7 +200,7 @@
         for k in range(n_half):
             for part in (1, 0):
                 for way in range(2):
-                    block = farthest(way, step, k)
+                    block = farthest(way, step * n_half + k)
 
                     @pl.when((first if way == 0 else last) & (fo != block))
                     def _():
@@ -218,34 +219,37 @@
                 total.astype(jnp.bfloat16).reshape(2, 2, 2, rows, lanes))
         near(a).start()
 
-    def farthest(way, step, k):
-        return n_fo - 1 - step * n_half - k if way == 0 else step * n_half + k
+    def farthest(way, k):
+        return n_fo - 1 - k if way == 0 else k
 
     def grad(w, c, block, part, way, src=None):
         held = g_in.at[way, w, c, block, part]
         return remote(held if src is None else src, held, zr_send.at[way, w, c, block, part],
                       zr_recv.at[way, w, c, block, part], ahead(way), tp)
 
-    def carry(w, c, step, k):
-        for part in (1, 0):
+    def carry(c, start, stop):
+        def position(q, carried):
             for way in range(2):
-                block = farthest(way, step, k)
-                inside = (fo < block) & (fo > 0) if way == 0 else (fo > block) & (fo < n_fo - 1)
-
-                @pl.when(inside)
+                hop = fo if way == 0 else n_fo - 1 - fo
+                item = q - SKEW * (hop - 1)
+                w = 1 - item // (2 * n_fo)
+                block = farthest(way, item % (2 * n_fo) // 2)
+                part = 1 - item % 2
+                inside = (hop > 0) & (hop < n_fo - 1) & (item >= 0) & (item < 4 * n_fo)
+                beyond = fo < block if way == 0 else fo > block
+
+                @pl.when(inside & beyond)
                 def _():
+                    row = jnp.where(part == 1, 1 - fi, fi)
                     grad(w, c, block, part, way).wait_recv()
                     g_in[way, w, c, block, part] = (
-                        g_out[w, c, block, side(part)].astype(jnp.float32)
+                        g_out[w, c, block, row].astype(jnp.float32)
                         + g_in[way, w, c, block, part].astype(jnp.float32)
                     ).astype(jnp.bfloat16)
                     grad(w, c, block, part, way).start()
-
-    def carry_all(c):
-        for step in range(2):
-            for w in (DOWN, UP):
-                for k in range(n_half):
-                    carry(w, c, step, k)
+            return carried
+
+        lax.fori_loop(start, stop, position, 0)
 
     def swap(w, c):
         return remote(staged.at[w, c], other.at[w, c], x_send.at[w, c], x_recv.at[w, c], pair, tp)
@@ -280,10 +284,18 @@
     def near(a):
         return remote(partial.at[a, :, :, 1 - core], landed.at[a], c_send.at[a], c_recv.at[a], fs, sibling)
 
-    def far(a, k):
-        at_fi, at_y = spot(k)
-        return remote(pair_sum.at[a, at_fi, at_y], arrived.at[a, k - 1], p_send.at[a, k], p_recv.at[a, k],
-                      fo * 2 + at_fi, at_y * 2 + core)
+    near_rows, far_rows = pl.ds(0, fold), pl.ds(fold, rows - fold)
+
+    def far(a, j):
+        to_x = j in (0, 1, 5)
+        lines = near_rows if j in (0, 1, 4) else far_rows
+        if j < 4:
+            src = pair_sum.at[a, *spot({0: 1, 1: 3, 2: 2, 3: 3}[j]), lines]
+            dst = arrived.at[a, j % 2, lines]
+        else:
+            src = arrived.at[a, 1, lines]
+            dst = arrived.at[a, 2, lines]
+        return remote(src, dst, p_send.at[a, j], p_recv.at[a, j], pair if to_x else fs, tp if to_x else across_y)
 
     def joined(a, at_fi, at_y):
         return (partial[a, at_fi, at_y, core].astype(jnp.float32)
@@ -291,16 +303,24 @@
 
     def spread(a):
         near(a).wait_recv()
-        for k in (3, 1, 2):
-            at_fi, at_y = spot(k)
-            pair_sum[a, at_fi, at_y] = joined(a, at_fi, at_y).astype(jnp.bfloat16)
-            far(a, k).start()
+        for k, sends in ((3, (1, 3)), (1, (0,)), (2, (2,))):
+            pair_sum[(a, *spot(k))] = joined(a, *spot(k)).astype(jnp.bfloat16)
+            for j in sends:
+                far(a, j).start()
+
+    def relay(a):
+        for j, k, lines in ((1, 2, near_rows), (3, 1, far_rows)):
+            far(a, j).wait_recv()
+            arrived[a, 1, lines] = (
+                pair_sum[(a, *spot(k), lines)].astype(jnp.float32)
+                + arrived[a, 1, lines].astype(jnp.float32)
+            ).astype(jnp.bfloat16)
+            far(a, j // 2 + 4).start()
 
     def collect(a):
-        total = joined(a, fi, y)
-        for k in (1, 2, 3):
-            far(a, k).wait_recv()
-            total += arrived[a, k - 1].astype(jnp.float32)
+        for j in (0, 2, 4, 5):
+            far(a, j).wait_recv()
+        total = joined(a, fi, y) + arrived[a, 0].astype(jnp.float32) + arrived[a, 2].astype(jnp.float32)
         summed[a][...] = total.astype(jnp.bfloat16)
 
     barrier = pltpu.get_barrier_semaphore()
@@ -311,24 +331,19 @@
     greet(pair, tp)
     greet(fs, across_y)
     greet(fs, sibling)
-    greet(pair, across_y)
     for way in range(2):
         @pl.when(open_way(way))
         def _():
             greet(ahead(way), tp)
-    pl.semaphore_wait(barrier, 4 + (fo > 0).astype(jnp.int32) + (fo < n_fo - 1).astype(jnp.int32))
-
-    for way in range(2):
-        @pl.when(open_way(way))
-        def _():
-            begin(0, way)
-    for w in range(2):
-        across(w, 0).start()
+    pl.semaphore_wait(barrier, 3 + (fo > 0).astype(jnp.int32) + (fo < n_fo - 1).astype(jnp.int32))
+
+    begin(UP, 0)
+    across(UP, 0).start()
     for a in (EARLY, COT):
         token(a, 0).start()
         token(a, 1).start()
-    for w in range(2):
-        across(w, 1).start()
+        if a == EARLY:
+            across(DOWN, 0).start()
     for a in (EARLY, COT, LATE):
         token(a, 4).start()
     own = [pltpu.make_async_copy(tokens[a], slot(a, 0, core), local.at[a]) for a in range(3)]
@@ -338,89 +353,105 @@
         copy.start()
 
     inner = range(2, n_fo - 1)
-    forward(0, 0, 1)
-    crossed(0)
-    begin_after(1, 0)
+    crossed(UP, 0)
+    begin(DOWN, 0, 0)
+    forward(UP, 0, 0, 1)
     from_y(EARLY)
+    for w in (UP, DOWN):
+        across(w, 1).start()
+    forward_far(UP, 0, 0)
+    forward(UP, 0, 1, 1)
+    begin(DOWN, 0, 1)
+    from_x(EARLY)
     for distance in inner:
-        forward(0, 0, distance)
-    from_x(EARLY)
-    forward(0, 1, 1)
-    begin_after(1, 1)
+        forward(UP, 0, 1, distance)
+        begin(DOWN, 0, distance)
+    crossed(DOWN, 0)
+    for w in (UP, DOWN):
+        begin(w, 1, 0)
+    forward(DOWN, 0, 0, 1)
     from_y(COT)
-    for distance in inner:
-        forward(0, 1, distance)
-        begin_after(1, distance)
+    forward_far(DOWN, 0, 0)
+    forward(DOWN, 0, 1, 1)
+    begin(UP, 1, 1)
     from_x(COT)
     token(LATE, 0).start()
     token(LATE, 1).start()
+    for distance in inner:
+        forward(DOWN, 0, 1, distance)
+        begin(UP, 1, distance)
     diagonal(EARLY)
-    forward(1, 0, 1)
-    crossed(1)
-    diagonal(COT)
     for copy in own:
         copy.wait()
     from_sibling(EARLY)
+    settle(UP, 0)
+    crossed(UP, 1)
+    forward(UP, 1, 0, 1)
+    activate(0)
+    crossed(DOWN, 1)
+    forward_far(UP, 1, 0)
+    diagonal(COT)
+    forward(UP, 1, 1, 1)
+    begin(DOWN, 1, 1)
     from_sibling(COT)
-    settle(0)
-
-    activate(0)
     weight_grad(DOWN, 0, 0)
+    weight_grad(DOWN, 0, 1)
+    settle(DOWN, 0)
+    hidden_grad(0)
     for distance in inner:
-        forward(1, 0, distance)
-    hidden_grad(0)
+        forward(UP, 1, 1, distance)
+        begin(DOWN, 1, distance)
     weight_grad(UP, 0, 0)
-    forward(1, 1, 1)
-    weight_grad(DOWN, 0, 1)
     weight_grad(UP, 0, 1)
+    forward(DOWN, 1, 0, 1)
     from_y(LATE)
     from_x(LATE)
-    for k in range(n_half):
-        carry(DOWN, 0, 0, k)
-        if k == 0:
-            for distance in inner:
-                forward(1, 1, distance)
-            diagonal(LATE)
+    forward_far(DOWN, 1, 0)
+    carry(0, 0, 1)
+    forward(DOWN, 1, 1, 1)
+    carry(0, 1, 2)
+    forward_far(DOWN, 1, 1)
+    carry(0, 2, n_fo)
+    diagonal(LATE)
+    carry(0, n_fo, n_fo + 1)
     from_sibling(LATE)
     activate_late(0)
-    for k in range(n_half):
-        carry(UP, 0, 0, k)
-    for w in (DOWN, UP):
-        for k in range(n_half):
-            carry(w, 0, 1, k)
-
-    settle(1)
+    carry(0, n_fo + 1, 2 * n_fo)
+    settle(UP, 1)
     activate(1)
     weight_grad(DOWN, 1, 0)
+    weight_grad(DOWN, 1, 1)
+    carry(0, 2 * n_fo, 2 * n_fo + 2)
+    activate_late(1)
+    carry(0, 2 * n_fo + 2, 4 * n_fo + SKEW * (n_fo - 3))
+    settle(DOWN, 1)
     hidden_grad(1)
+    token_partial(1, 1, UP)
     weight_grad(UP, 1, 0)
-    weight_grad(DOWN, 1, 1)
-    weight_grad(UP, 1, 1)
-    token_partial(1, 1, UP)
-    activate_late(1)
     spread(1)
     token_partial(0, 2, DOWN)
-    for k in range(n_half):
-        carry(DOWN, 1, 0, k)
-        if k == 0:
-            spread(0)
-            for w in (DOWN, UP):
-                owned(w, 0, 1)
-    for k in range(n_half):
-        carry(UP, 1, 0, k)
-    for w in (DOWN, UP):
-        for k in range(n_half):
-            carry(w, 1, 1, k)
-    for w in (DOWN, UP):
-        owned(w, 0, 0)
+    weight_grad(UP, 1, 1)
+    spread(0)
+    owned(DOWN, 0, 1)
+    owned(DOWN, 0, 0)
+    carry(1, 0, 1)
+    relay(1)
+    carry(1, 1, 2)
+    owned(UP, 0, 1)
+    owned(UP, 0, 0)
+    carry(1, 2, n_fo)
+    relay(0)
+    carry(1, n_fo, 2 * n_fo)
     for w in (DOWN, UP):
         swapped(w, 0)
+    carry(1, 2 * n_fo, 2 * n_fo + SKEW)
     owned(DOWN, 1, 1)
     owned(DOWN, 1, 0)
+    carry(1, 2 * n_fo + SKEW, 4 * n_fo + SKEW * (n_fo - 3))
     collect(1)
+    collect(0)
     owned(UP, 1, 1)
     owned(UP, 1, 0)
-    collect(0)
     for w in (DOWN, UP):
         swapped(w, 1)
 
@@ -452,8 +483,8 @@
                             grad(w, c, block, part, way).wait_send()
     for a in range(2):
         near(a).wait_send()
-        for k in (1, 2, 3):
-            far(a, k).wait_send()
+        for j in range(6):
+            far(a, j).wait_send()
 
 
 def layer(n_fo, n_tp, tokens, weights):
@@ -484,12 +515,12 @@
             pltpu.VMEM((2, CHUNKS, w_rows, wide), bf16),
             dma((3 + 2 * CHUNKS,)), dma((3, 8)), dma((3, 8)), dma((2, CHUNKS)), dma((2, CHUNKS)),
             dma((2, 2, CHUNKS, n_fo, 2)), dma((2, CHUNKS, n_fo, 2)),
-            dma((2,)), dma((2,)), dma((2, 4)), dma((2, 4)),
+            dma((2,)), dma((2,)), dma((2, 6)), dma((2, 6)),
             dma((2, 2, CHUNKS, n_fo, 2)), dma((2, 2, CHUNKS, n_fo, 2)),
             dma((2, CHUNKS)), dma((2, CHUNKS)),
         ],
         compiler_params=pltpu.CompilerParams(
-            collective_id=0, has_side_effects=True, vmem_limit_bytes=64_000_000),
+            collective_id=0, has_side_effects=True, vmem_limit_bytes=52_000_000),
         name="layer",
     )(*tokens, *weights)
 

time: 167 us -> 139 us (0.83); the launches traced: 166 us -> 136 us
  Pallas kernels: 160 us -> 126 us
  local copies, waits for them, and re-layouts: 1.9 us -> 7.31 us
    pallas_call x1, Pallas kernels: 160 us -> 126 us  [layer(): pl.pallas_call(functools.partial(layer_kernel, n_fo, n_tp), out_shape=[ja...]
    unnamed x12 -> x18, local copies, waits for them, and re-layouts: 1.9 us -> 7.31 us
where the time goes in v2:
time: 139 us; the launch traced here: 136 us
  Pallas kernels  126 us (91%)
  local copies, waits for them, and re-layouts  7.31 us (5%)
  other arithmetic  2.26 us (2%)
    pallas_call x1, Pallas kernels, layer(): pl.pallas_call(functools.partial(layer_kernel, n_fo, n_tp), out_shape=[ja...  126 us
    unnamed x18, local copies, waits for them, and re-layouts  7.31 us

profile of v2, /device:TPU:0, one launch (start us, length us, event | category | flops | bytes accessed | tf_op | source)
XLA Modules:
  0.0 136.2 jit_solution(16576817764161286479)
XLA Ops:
  0.6 0.0 copy-start
  0.6 1.0 copy-done
  1.7 0.0 copy-start.1
  1.7 1.0 copy-done.1
  2.7 0.0 copy-start.2
  2.7 1.0 copy-done.2
  3.7 0.0 copy-start.3
  3.7 1.0 copy-done.3
  4.7 0.0 copy-start.4
  4.7 1.0 copy-done.4
  5.7 0.0 copy-start.5
  5.7 126.0 %layer.1 = (bf16[96,2048]{1,0:T(8,128)(2,1)S(1)}, bf16[96,2048]{1,0:T(8,128)(2,1)S(1)}, f32[256,1024]{1,0:T(8,128)S(1)}, f32[256,1024]{1,0:T(8,128)}) custom-call(bf16[96,2048]{1,0:T(8,128)(2,1)S(1)} %copy-done.2, bf16[96,2048]{1,0:T(8,128)(2,1)S(1)} %copy-done.3, bf16[96,2048]{1,0:T(8,128)(2,1)S(1)} %copy-done.4, bf16[256,1024]{1,0:T(8,128)(2,1)S(1)} %copy-done, ...), custom_call_target="tpu_custom_call" | custom-call | tf_op jit(solution)/shard_map/layer/pallas_call | solution.py:497
  131.7 0.0 copy-done.5
  131.7 0.0 copy-start.6
  131.7 0.0 copy-start.7
  131.7 1.2 add.6
  132.9 0.3 copy-done.6
  133.2 0.5 copy-done.7
  133.6 1.1 add.7
  134.7 0.7 copy.13
  135.5 0.7 copy.14
Async XLA Ops:
  0.6 1.0 copy-start
  1.7 1.0 copy-start.1
  2.7 1.0 copy-start.2
  3.7 1.0 copy-start.3
  4.7 1.0 copy-start.4
  5.7 126.0 %copy-start.5 = (f32[256,1024]{1,0:T(8,128)S(1)}, f32[256,1024]{1,0:T(8,128)}, u32[]{:S(2)}) copy-start(f32[256,1024]{1,0:T(8,128)} %param.12) | copy-start | bytes 3145732
  131.7 1.5 %copy-start.6 = (f32[256,1024]{1,0:T(8,128)S(1)}, f32[256,1024]{1,0:T(8,128)}, u32[]{:S(2)}) copy-start(f32[256,1024]{1,0:T(8,128)} %param.13) | copy-start | bytes 3145732
  131.7 1.9 %copy-start.7 = (f32[256,1024]{1,0:T(8,128)S(1)}, f32[256,1024]{1,0:T(8,128)}, u32[]{:S(2)}) copy-start(f32[256,1024]{1,0:T(8,128)} %get-tuple-element.11) | copy-start | bytes 3145732

commit v3 on v2

--- a/solution.py
+++ b/solution.py
@@ -10,6 +10,7 @@
 
 MESH = pl.DeviceIdType.MESH
 VMEM = pl.BlockSpec(memory_space=pltpu.VMEM)
+HBM = pl.BlockSpec(memory_space=pltpu.HBM)
 EARLY, COT, LATE = 0, 1, 2
 UP, DOWN = 0, 1
 CHUNKS = 2
@@ -32,7 +33,7 @@
 def layer_kernel(n_fo, n_tp, *refs):
     tokens, weights = refs[0:3], refs[3:5]
     summed, grads = refs[5:7], refs[7:9]
-    (tok, wts, g_out, g_in, pre, hid, partial, landed, pair_sum, arrived, staged, other,
+    (tok, wts, lent, g_out, g_in, pre, hid, partial, landed, pair_sum, arrived, staged, other,
      local, t_send, t_recv, a_send, a_recv, zg_send, zg_recv,
      c_send, c_recv, p_send, p_recv, zr_send, zr_recv, x_send, x_recv) = refs[9:]
     fs, tp = lax.axis_index("fs"), lax.axis_index("tp")
@@ -47,7 +48,7 @@
     wide = half // CHUNKS
     count = 4 * rows * 2
     cut = rows // 96 * 16
-    fold = rows // 96 * 32
+    fold = rows // 96 * 16
     first, last = fo == 0, fo == n_fo - 1
 
     def side(part):
@@ -68,9 +69,9 @@
     def token(a, j):
         sems = t_send.at[a, j], t_recv.at[a, j]
         if j == 0:
-            return remote(tokens[a], slot(a, 0, core), *sems, pair, tp)
+            return remote(slot(a, 0, core), slot(a, 0, core), *sems, pair, tp)
         if j == 1:
-            return remote(tokens[a], slot(a, 0, core), *sems, fs, across_y)
+            return remote(slot(a, 0, core), slot(a, 0, core), *sems, fs, across_y)
         if j == 2:
             part = slot(a, 2, core).at[pl.ds(0, cut)]
             return remote(part, part, *sems, pair, tp)
@@ -79,7 +80,7 @@
             return remote(part, part, *sems, fs, across_y)
         k = j - 4
         dst = slot(a, k, core)
-        return remote(tokens[a] if k == 0 else dst, dst, *sems, fs, sibling)
+        return remote(dst, dst, *sems, fs, sibling)
 
     def token_in(a, j):
         sems = t_send.at[a, j], t_recv.at[a, j]
@@ -115,16 +116,24 @@
     def columns(w, which, c):
         return weights[w].at[:, pl.ds(pl.multiple_of(which * half + c * wide, wide), wide)]
 
+    def load_tokens(a):
+        return pltpu.make_async_copy(tokens[a], slot(a, 0, core), local.at[a])
+
+    def load_weight(w, c, mine):
+        dst = wts.at[w, c, fo, fi] if mine else lent.at[w, c]
+        sem = local.at[3 + (w * CHUNKS + c) * 2 + mine]
+        return pltpu.make_async_copy(columns(w, fi if mine else 1 - fi, c), dst, sem)
+
     def across(w, c):
-        return remote(columns(w, 1 - fi, c), wts.at[w, c, fo, fi], a_send.at[w, c], a_recv.at[w, c], pair, tp)
+        return remote(lent.at[w, c], wts.at[w, c, fo, fi], a_send.at[w, c], a_recv.at[w, c], pair, tp)
 
     def across_in(w, c):
         dst = wts.at[w, c, fo, 1 - fi]
         return remote(dst, dst, a_send.at[w, c], a_recv.at[w, c], pair, tp)
 
-    def along(w, c, source, part, way, src=None):
+    def along(w, c, source, part, way):
         dst = wts.at[w, c, source, side(part)]
-        return remote(dst if src is None else src, dst, zg_send.at[way, w, c, source, part],
+        return remote(dst, dst, zg_send.at[way, w, c, source, part],
                       zg_recv.at[w, c, source, part], ahead(way), tp)
 
     def begin(w, c, distance=None):
@@ -133,7 +142,7 @@
 
             @pl.when(open_way(way) if distance is None else open_way(way) & (behind == distance))
             def _():
-                along(w, c, fo, 0, way, columns(w, fi, c)).start()
+                along(w, c, fo, 0, way).start()
 
     def crossed(w, c):
         across_in(w, c).wait_recv()
@@ -206,18 +215,20 @@
                     def _():
                         grad(w, c, block, part, way, g_out.at[w, c, block, side(part)]).start()
 
+    def token_begin(a, h, w):
+        value = dot(hid[h, 0], weight(w, 0), 1, 1)
+        partial[a] = value.astype(jnp.bfloat16).reshape(2, 2, 2, rows, width)
+
     def token_partial(a, h, w):
-        sources = max(1, 512 // (2 * w_rows))
-        lanes = sources * 2 * w_rows
-        for b in range(n_fo // sources):
-            total = None
-            for c in range(CHUNKS):
-                right = wts[w, c, b * sources:(b + 1) * sources].reshape(lanes, wide)
-                term = dot(hid[h, c], right, 1, 1)
-                total = term if total is None else total + term
-            partial[a, :, :, :, :, b * lanes:(b + 1) * lanes] = (
-                total.astype(jnp.bfloat16).reshape(2, 2, 2, rows, lanes))
-        near(a).start()
+        for dx, spots_of in ((1, (3, 1)), (0, (2, 0))):
+            at_fi = 1 - fi if dx else fi
+            lines = pl.ds(pl.multiple_of(at_fi * 4 * rows, 4 * rows), 4 * rows)
+            total = partial[a, at_fi].astype(jnp.float32).reshape(4 * rows, width)
+            for c in range(1, CHUNKS):
+                total += dot(hid[h, c, lines], weight(w, c), 1, 1)
+            partial[a, at_fi] = total.astype(jnp.bfloat16).reshape(2, 2, rows, width)
+            for k in spots_of:
+                near(a, k).start()
 
     def farthest(way, k):
         return n_fo - 1 - k if way == 0 else k
@@ -281,8 +292,9 @@
         dx, dy = spots[k]
         return (1 - fi if dx else fi), (1 - y if dy else y)
 
-    def near(a):
-        return remote(partial.at[a, :, :, 1 - core], landed.at[a], c_send.at[a], c_recv.at[a], fs, sibling)
+    def near(a, k):
+        return remote(partial.at[(a, *spot(k), 1 - core)], landed.at[(a, *spot(k))], c_send.at[a, k],
+                      c_recv.at[a, k], fs, sibling)
 
     near_rows, far_rows = pl.ds(0, fold), pl.ds(fold, rows - fold)
 
@@ -301,9 +313,9 @@
         return (partial[a, at_fi, at_y, core].astype(jnp.float32)
                 + landed[a, at_fi, at_y].astype(jnp.float32))
 
-    def spread(a):
-        near(a).wait_recv()
-        for k, sends in ((3, (1, 3)), (1, (0,)), (2, (2,))):
+    def spread(a, diagonal_spot):
+        for k, sends in ((3, (1, 3)),) if diagonal_spot else ((1, (0,)), (2, (2,))):
+            near(a, k).wait_recv()
             pair_sum[(a, *spot(k))] = joined(a, *spot(k)).astype(jnp.bfloat16)
             for j in sends:
                 far(a, j).start()
@@ -318,6 +330,7 @@
             far(a, j // 2 + 4).start()
 
     def collect(a):
+        near(a, 0).wait_recv()
         for j in (0, 2, 4, 5):
             far(a, j).wait_recv()
         total = joined(a, fi, y) + arrived[a, 0].astype(jnp.float32) + arrived[a, 2].astype(jnp.float32)
@@ -335,41 +348,44 @@
         @pl.when(open_way(way))
         def _():
             greet(ahead(way), tp)
+    for c in range(CHUNKS):
+        for w in (UP, DOWN):
+            for mine in (True, False):
+                load_weight(w, c, mine).start()
+        load_tokens(EARLY + c).start()
+    load_tokens(LATE).start()
     pl.semaphore_wait(barrier, 3 + (fo > 0).astype(jnp.int32) + (fo < n_fo - 1).astype(jnp.int32))
 
-    begin(UP, 0)
-    across(UP, 0).start()
-    for a in (EARLY, COT):
-        token(a, 0).start()
-        token(a, 1).start()
-        if a == EARLY:
-            across(DOWN, 0).start()
+    for w in (UP, DOWN):
+        load_weight(w, 0, True).wait()
+        load_weight(w, 0, False).wait()
+        begin(w, 0)
+        across(w, 0).start()
+        load_tokens(EARLY + w).wait()
+        token(EARLY + w, 1).start()
+        token(EARLY + w, 0).start()
+    load_tokens(LATE).wait()
     for a in (EARLY, COT, LATE):
         token(a, 4).start()
-    own = [pltpu.make_async_copy(tokens[a], slot(a, 0, core), local.at[a]) for a in range(3)]
-    own += [pltpu.make_async_copy(columns(w, fi, c), wts.at[w, c, fo, fi], local.at[3 + w * CHUNKS + c])
-            for w in range(2) for c in range(CHUNKS)]
-    for copy in own:
-        copy.start()
+    for w in (UP, DOWN):
+        for mine in (True, False):
+            load_weight(w, 1, mine).wait()
 
     inner = range(2, n_fo - 1)
     crossed(UP, 0)
-    begin(DOWN, 0, 0)
     forward(UP, 0, 0, 1)
     from_y(EARLY)
     for w in (UP, DOWN):
         across(w, 1).start()
     forward_far(UP, 0, 0)
     forward(UP, 0, 1, 1)
-    begin(DOWN, 0, 1)
     from_x(EARLY)
     for distance in inner:
         forward(UP, 0, 1, distance)
-        begin(DOWN, 0, distance)
+    forward(DOWN, 0, 0, 1)
     crossed(DOWN, 0)
     for w in (UP, DOWN):
         begin(w, 1, 0)
-    forward(DOWN, 0, 0, 1)
     from_y(COT)
     forward_far(DOWN, 0, 0)
     forward(DOWN, 0, 1, 1)
@@ -381,79 +397,81 @@
         forward(DOWN, 0, 1, distance)
         begin(UP, 1, distance)
     diagonal(EARLY)
-    for copy in own:
-        copy.wait()
     from_sibling(EARLY)
     settle(UP, 0)
+    forward(UP, 1, 0, 1)
     crossed(UP, 1)
-    forward(UP, 1, 0, 1)
     activate(0)
     crossed(DOWN, 1)
-    forward_far(UP, 1, 0)
-    diagonal(COT)
     forward(UP, 1, 1, 1)
     begin(DOWN, 1, 1)
+    diagonal(COT)
     from_sibling(COT)
     weight_grad(DOWN, 0, 0)
     weight_grad(DOWN, 0, 1)
+    forward(DOWN, 1, 0, 1)
+    forward_far(UP, 1, 0)
     settle(DOWN, 0)
     hidden_grad(0)
     for distance in inner:
         forward(UP, 1, 1, distance)
         begin(DOWN, 1, distance)
+    from_y(LATE)
+    from_x(LATE)
     weight_grad(UP, 0, 0)
     weight_grad(UP, 0, 1)
-    forward(DOWN, 1, 0, 1)
-    from_y(LATE)
-    from_x(LATE)
+    forward(DOWN, 1, 1, 1)
+    carry(0, 0, 2)
     forward_far(DOWN, 1, 0)
-    carry(0, 0, 1)
-    forward(DOWN, 1, 1, 1)
-    carry(0, 1, 2)
+    carry(0, 2, 3)
     forward_far(DOWN, 1, 1)
-    carry(0, 2, n_fo)
     diagonal(LATE)
-    carry(0, n_fo, n_fo + 1)
+    carry(0, 3, n_fo)
     from_sibling(LATE)
     activate_late(0)
-    carry(0, n_fo + 1, 2 * n_fo)
+    token_begin(0, 2, DOWN)
+    carry(0, n_fo, 2 * n_fo + 2)
+    token_begin(1, 1, UP)
     settle(UP, 1)
     activate(1)
+    carry(0, 2 * n_fo + 2, 2 * n_fo + 3)
     weight_grad(DOWN, 1, 0)
     weight_grad(DOWN, 1, 1)
-    carry(0, 2 * n_fo, 2 * n_fo + 2)
+    carry(0, 2 * n_fo + 3, 4 * n_fo + SKEW * (n_fo - 3))
     activate_late(1)
-    carry(0, 2 * n_fo + 2, 4 * n_fo + SKEW * (n_fo - 3))
     settle(DOWN, 1)
+    token_partial(0, 2, DOWN)
+    spread(0, True)
     hidden_grad(1)
+    carry(1, 0, 1)
     token_partial(1, 1, UP)
+    spread(1, True)
+    carry(1, 1, 2)
+    spread(0, False)
+    owned(DOWN, 0, 1)
     weight_grad(UP, 1, 0)
-    spread(1)
-    token_partial(0, 2, DOWN)
+    carry(1, 2, 3)
+    spread(1, False)
     weight_grad(UP, 1, 1)
-    spread(0)
-    owned(DOWN, 0, 1)
-    owned(DOWN, 0, 0)
-    carry(1, 0, 1)
-    relay(1)
-    carry(1, 1, 2)
     owned(UP, 0, 1)
-    owned(UP, 0, 0)
-    carry(1, 2, n_fo)
+    carry(1, 3, n_fo)
     relay(0)
     carry(1, n_fo, 2 * n_fo)
     for w in (DOWN, UP):
-        swapped(w, 0)
-    carry(1, 2 * n_fo, 2 * n_fo + SKEW)
+        owned(w, 0, 0)
+    relay(1)
+    carry(1, 2 * n_fo, 2 * n_fo + 1)
     owned(DOWN, 1, 1)
     owned(DOWN, 1, 0)
-    carry(1, 2 * n_fo + SKEW, 4 * n_fo + SKEW * (n_fo - 3))
+    carry(1, 2 * n_fo + 1, 4 * n_fo + SKEW * (n_fo - 3))
+    for w in (DOWN, UP):
+        swapped(w, 0)
+    owned(UP, 1, 1)
+    collect(0)
+    owned(UP, 1, 0)
+    swapped(DOWN, 1)
     collect(1)
-    collect(0)
-    owned(UP, 1, 1)
-    owned(UP, 1, 0)
-    for w in (DOWN, UP):
-        swapped(w, 1)
+    swapped(UP, 1)
 
     for a in range(3):
         for j in range(8):
@@ -482,7 +500,8 @@
                         for part in range(2):
                             grad(w, c, block, part, way).wait_send()
     for a in range(2):
-        near(a).wait_send()
+        for k in range(4):
+            near(a, k).wait_send()
         for j in range(6):
             far(a, j).wait_send()
 
@@ -498,11 +517,12 @@
         functools.partial(layer_kernel, n_fo, n_tp),
         out_shape=[jax.ShapeDtypeStruct((rows, width), bf16)] * 2
         + [jax.ShapeDtypeStruct((w_rows, cols), f32)] * 2,
-        in_specs=[VMEM] * 5,
+        in_specs=[HBM] * 5,
         out_specs=[VMEM] * 4,
         scratch_shapes=[
             pltpu.VMEM((3, 2, 2, 2, rows, width), bf16),
             pltpu.VMEM((2, CHUNKS, n_fo, 2, w_rows, wide), bf16),
+            pltpu.VMEM((2, CHUNKS, w_rows, wide), bf16),
             pltpu.VMEM((2, CHUNKS, n_fo, 2, w_rows, wide), bf16),
             pltpu.VMEM((2, 2, CHUNKS, n_fo, 2, w_rows, wide), bf16),
             pltpu.VMEM((count, wide), f32),
@@ -513,16 +533,16 @@
             pltpu.VMEM((2, 3, rows, width), bf16),
             pltpu.VMEM((2, CHUNKS, w_rows, wide), bf16),
             pltpu.VMEM((2, CHUNKS, w_rows, wide), bf16),
-            dma((3 + 2 * CHUNKS,)), dma((3, 8)), dma((3, 8)), dma((2, CHUNKS)), dma((2, CHUNKS)),
+            dma((3 + 4 * CHUNKS,)), dma((3, 8)), dma((3, 8)), dma((2, CHUNKS)), dma((2, CHUNKS)),
             dma((2, 2, CHUNKS, n_fo, 2)), dma((2, CHUNKS, n_fo, 2)),
-            dma((2,)), dma((2,)), dma((2, 6)), dma((2, 6)),
+            dma((2, 4)), dma((2, 4)), dma((2, 6)), dma((2, 6)),
             dma((2, 2, CHUNKS, n_fo, 2)), dma((2, 2, CHUNKS, n_fo, 2)),
             dma((2, CHUNKS)), dma((2, CHUNKS)),
         ],
         compiler_params=pltpu.CompilerParams(
-            collective_id=0, has_side_effects=True, vmem_limit_bytes=52_000_000),
+            collective_id=0, has_side_effects=True, vmem_limit_bytes=50_000_000),
         name="layer",
-    )(*tokens, *weights)
+    )(*(pltpu.with_memory_space_constraint(a, pltpu.HBM) for a in (*tokens, *weights)))
 
 
 def on_device(n_fo, n_tp, x_late, x_early, cotangent, up_weight, down_weight, up_grad_sum, down_grad_sum):

time: 139 us -> 125 us (0.90); the launches traced: 136 us -> 125 us
  Pallas kernels: 126 us -> 120 us
  local copies, waits for them, and re-layouts: 7.31 us -> 1.82 us
    pallas_call x1, Pallas kernels: 126 us -> 120 us  [layer(): pl.pallas_call(functools.partial(layer_kernel, n_fo, n_tp), out_shape=[ja...]
    unnamed x18 -> x6, local copies, waits for them, and re-layouts: 7.31 us -> 1.82 us
where the time goes in v3:
time: 125 us
  Pallas kernels  120 us (96%)
  other arithmetic  2.26 us (2%)
  local copies, waits for them, and re-layouts  1.82 us (1%)
    pallas_call x1, Pallas kernels, layer(): pl.pallas_call(functools.partial(layer_kernel, n_fo, n_tp), out_shape=[ja...  120 us

profile of v3, /device:TPU:0, one launch (start us, length us, event | category | flops | bytes accessed | tf_op | source)
XLA Modules:
  0.0 125.1 jit_solution(4787345543107372581)
XLA Ops:
  0.6 0.0 copy-start
  0.6 120.4 %layer.1 = (bf16[96,2048]{1,0:T(8,128)(2,1)S(1)}, bf16[96,2048]{1,0:T(8,128)(2,1)S(1)}, f32[256,1024]{1,0:T(8,128)S(1)}, f32[256,1024]{1,0:T(8,128)S(1)}) custom-call(bf16[96,2048]{1,0:T(8,128)(2,1)} %refs_0_.1, bf16[96,2048]{1,0:T(8,128)(2,1)} %refs_1_.1, bf16[96,2048]{1,0:T(8,128)(2,1)} %refs_2_.1, bf16[256,1024]{1,0:T(8,128)(2,1)} %refs_3_.1, ...), custom_call_target="tpu_custom_call" | custom-call | tf_op jit(solution)/shard_map/layer/pallas_call | solution.py:516
  121.0 0.0 copy-done
  121.0 0.0 copy-start.1
  121.0 1.2 add.6
  122.2 0.3 copy-done.1
  122.5 1.1 add.7
  123.6 0.7 copy.13
  124.4 0.7 copy.14
Async XLA Ops:
  0.6 120.4 %copy-start = (f32[256,1024]{1,0:T(8,128)S(1)}, f32[256,1024]{1,0:T(8,128)}, u32[]{:S(2)}) copy-start(f32[256,1024]{1,0:T(8,128)} %param.12) | copy-start | bytes 3145732
  121.0 1.5 %copy-start.1 = (f32[256,1024]{1,0:T(8,128)S(1)}, f32[256,1024]{1,0:T(8,128)}, u32[]{:S(2)}) copy-start(f32[256,1024]{1,0:T(8,128)} %param.13) | copy-start | bytes 3145732

commit v4 on v3

--- a/solution.py
+++ b/solution.py
@@ -67,7 +67,7 @@
         return tok.at[a, (1 - fi if dx else fi), (1 - y if dy else y), at_core]
 
     def token(a, j):
-        sems = t_send.at[a, j], t_recv.at[a, j]
+        sems = t_send.at[a % 2, j], t_recv.at[a, j]
         if j == 0:
             return remote(slot(a, 0, core), slot(a, 0, core), *sems, pair, tp)
         if j == 1:
@@ -83,7 +83,7 @@
         return remote(dst, dst, *sems, fs, sibling)
 
     def token_in(a, j):
-        sems = t_send.at[a, j], t_recv.at[a, j]
+        sems = t_send.at[a % 2, j], t_recv.at[a, j]
         if j < 2:
             dst = slot(a, 1 + j, core)
         elif j == 2:
@@ -94,20 +94,25 @@
             dst = slot(a, j - 4, 1 - core)
         return remote(dst, dst, *sems, fs, sibling)
 
+    def send_token(a, j):
+        if a == LATE:
+            token(EARLY, j).wait_send()
+        token(a, j).start()
+
     def from_y(a):
         token_in(a, 1).wait_recv()
-        token(a, 2).start()
-        token(a, 6).start()
+        send_token(a, 2)
+        send_token(a, 6)
 
     def from_x(a):
         token_in(a, 0).wait_recv()
-        token(a, 3).start()
-        token(a, 5).start()
+        send_token(a, 3)
+        send_token(a, 5)
 
     def diagonal(a):
         token_in(a, 3).wait_recv()
         token_in(a, 2).wait_recv()
-        token(a, 7).start()
+        send_token(a, 7)
 
     def from_sibling(a):
         for k in range(4):
@@ -133,8 +138,13 @@
 
     def along(w, c, source, part, way):
         dst = wts.at[w, c, source, side(part)]
-        return remote(dst, dst, zg_send.at[way, w, c, source, part],
-                      zg_recv.at[w, c, source, part], ahead(way), tp)
+        sem = jnp.where(source == fo, n_fo, source) if way else source
+        return remote(dst, dst, zg_send.at[w, sem, part], zg_recv.at[w, c, source, part], ahead(way), tp)
+
+    def send_along(w, c, source, part, way):
+        if c:
+            along(w, c - 1, source, part, way).wait_send()
+        along(w, c, source, part, way).start()
 
     def begin(w, c, distance=None):
         for way in range(2):
@@ -142,14 +152,14 @@
 
             @pl.when(open_way(way) if distance is None else open_way(way) & (behind == distance))
             def _():
-                along(w, c, fo, 0, way).start()
+                send_along(w, c, fo, 0, way)
 
     def crossed(w, c):
         across_in(w, c).wait_recv()
         for way in range(2):
             @pl.when(open_way(way))
             def _():
-                along(w, c, fo, 1, way).start()
+                send_along(w, c, fo, 1, way)
 
     def incoming(way, distance):
         source = fo - distance if way == 0 else fo + distance
@@ -162,7 +172,7 @@
             @pl.when(inside & open_way(way))
             def _():
                 along(w, c, source, part, way).wait_recv()
-                along(w, c, source, part, way).start()
+                send_along(w, c, source, part, way)
 
     def forward_far(w, c, part):
         for distance in range(2, n_fo - 1):
@@ -213,7 +223,7 @@
 
                     @pl.when((first if way == 0 else last) & (fo != block))
                     def _():
-                        grad(w, c, block, part, way, g_out.at[w, c, block, side(part)]).start()
+                        send_grad(w, c, block, part, way, g_out.at[w, c, block, side(part)])
 
     def token_begin(a, h, w):
         value = dot(hid[h, 0], weight(w, 0), 1, 1)
@@ -233,10 +243,17 @@
     def farthest(way, k):
         return n_fo - 1 - k if way == 0 else k
 
-    def grad(w, c, block, part, way, src=None):
+    def grad(w, c, block, part, way, src=None, taker=None):
         held = g_in.at[way, w, c, block, part]
-        return remote(held if src is None else src, held, zr_send.at[way, w, c, block, part],
-                      zr_recv.at[way, w, c, block, part], ahead(way), tp)
+        taker = fo - 1 if taker is None else taker
+        sem = jnp.where(block == taker, n_fo, block) if way else block
+        return remote(held if src is None else src, held, zr_send.at[w, block, part],
+                      zr_recv.at[w, c, sem, part], ahead(way), tp)
+
+    def send_grad(w, c, block, part, way, src=None):
+        if c:
+            grad(w, c - 1, block, part, way, src).wait_send()
+        grad(w, c, block, part, way, src).start()
 
     def carry(c, start, stop):
         def position(q, carried):
@@ -252,12 +269,12 @@
                 @pl.when(inside & beyond)
                 def _():
                     row = jnp.where(part == 1, 1 - fi, fi)
-                    grad(w, c, block, part, way).wait_recv()
+                    grad(w, c, block, part, way, taker=fo).wait_recv()
                     g_in[way, w, c, block, part] = (
                         g_out[w, c, block, row].astype(jnp.float32)
                         + g_in[way, w, c, block, part].astype(jnp.float32)
                     ).astype(jnp.bfloat16)
-                    grad(w, c, block, part, way).start()
+                    send_grad(w, c, block, part, way)
             return carried
 
         lax.fori_loop(start, stop, position, 0)
@@ -273,7 +290,7 @@
 
             @pl.when(jnp.logical_not(first if way == 0 else last))
             def _():
-                grad(w, c, fo, part, way).wait_recv()
+                grad(w, c, fo, part, way, taker=fo).wait_recv()
         total = (g_out[w, c, fo, side(part)].astype(jnp.float32)
                  + g_in[0, w, c, fo, part].astype(jnp.float32)
                  + g_in[1, w, c, fo, part].astype(jnp.float32))
@@ -313,12 +330,11 @@
         return (partial[a, at_fi, at_y, core].astype(jnp.float32)
                 + landed[a, at_fi, at_y].astype(jnp.float32))
 
-    def spread(a, diagonal_spot):
-        for k, sends in ((3, (1, 3)),) if diagonal_spot else ((1, (0,)), (2, (2,))):
-            near(a, k).wait_recv()
-            pair_sum[(a, *spot(k))] = joined(a, *spot(k)).astype(jnp.bfloat16)
-            for j in sends:
-                far(a, j).start()
+    def spread(a, k):
+        near(a, k).wait_recv()
+        pair_sum[(a, *spot(k))] = joined(a, *spot(k)).astype(jnp.bfloat16)
+        for j in {3: (1, 3), 1: (0,), 2: (2,)}[k]:
+            far(a, j).start()
 
     def relay(a):
         for j, k, lines in ((1, 2, near_rows), (3, 1, far_rows)):
@@ -365,20 +381,20 @@
         token(EARLY + w, 1).start()
         token(EARLY + w, 0).start()
     load_tokens(LATE).wait()
-    for a in (EARLY, COT, LATE):
+    for a in (EARLY, COT):
         token(a, 4).start()
     for w in (UP, DOWN):
         for mine in (True, False):
             load_weight(w, 1, mine).wait()
 
     inner = range(2, n_fo - 1)
+    forward(UP, 0, 0, 1)
     crossed(UP, 0)
-    forward(UP, 0, 0, 1)
+    forward_far(UP, 0, 0)
+    forward(UP, 0, 1, 1)
     from_y(EARLY)
     for w in (UP, DOWN):
         across(w, 1).start()
-    forward_far(UP, 0, 0)
-    forward(UP, 0, 1, 1)
     from_x(EARLY)
     for distance in inner:
         forward(UP, 0, 1, distance)
@@ -391,8 +407,8 @@
     forward(DOWN, 0, 1, 1)
     begin(UP, 1, 1)
     from_x(COT)
-    token(LATE, 0).start()
-    token(LATE, 1).start()
+    for j in (0, 1, 4):
+        send_token(LATE, j)
     for distance in inner:
         forward(DOWN, 0, 1, distance)
         begin(UP, 1, distance)
@@ -441,17 +457,19 @@
     activate_late(1)
     settle(DOWN, 1)
     token_partial(0, 2, DOWN)
-    spread(0, True)
+    spread(0, 3)
     hidden_grad(1)
+    spread(0, 1)
     carry(1, 0, 1)
+    owned(DOWN, 0, 1)
     token_partial(1, 1, UP)
-    spread(1, True)
+    spread(1, 3)
     carry(1, 1, 2)
-    spread(0, False)
-    owned(DOWN, 0, 1)
+    spread(1, 1)
+    spread(0, 2)
     weight_grad(UP, 1, 0)
     carry(1, 2, 3)
-    spread(1, False)
+    spread(1, 2)
     weight_grad(UP, 1, 1)
     owned(UP, 0, 1)
     carry(1, 3, n_fo)
@@ -473,32 +491,33 @@
     collect(1)
     swapped(UP, 1)
 
-    for a in range(3):
+    for a in (COT, LATE):
         for j in range(8):
             token(a, j).wait_send()
     for w in range(2):
         for c in range(CHUNKS):
             across(w, c).wait_send()
             swap(w, c).wait_send()
-            for way in range(2):
-                @pl.when(open_way(way))
+        c = CHUNKS - 1
+        for way in range(2):
+            @pl.when(open_way(way))
+            def _():
+                for part in range(2):
+                    along(w, c, fo, part, way).wait_send()
+
+            for distance in range(1, n_fo):
+                source, inside = incoming(way, distance)
+
+                @pl.when(inside & open_way(way))
                 def _():
                     for part in range(2):
-                        along(w, c, fo, part, way).wait_send()
-
-                for distance in range(1, n_fo):
-                    source, inside = incoming(way, distance)
-
-                    @pl.when(inside & open_way(way))
-                    def _():
-                        for part in range(2):
-                            along(w, c, source, part, way).wait_send()
-
-                for block in range(n_fo):
-                    @pl.when(fo < block if way == 0 else fo > block)
-                    def _():
-                        for part in range(2):
-                            grad(w, c, block, part, way).wait_send()
+                        along(w, c, source, part, way).wait_send()
+
+            for block in range(n_fo):
+                @pl.when(fo < block if way == 0 else fo > block)
+                def _():
+                    for part in range(2):
+                        grad(w, c, block, part, way).wait_send()
     for a in range(2):
         for k in range(4):
             near(a, k).wait_send()
@@ -533,10 +552,10 @@
             pltpu.VMEM((2, 3, rows, width), bf16),
             pltpu.VMEM((2, CHUNKS, w_rows, wide), bf16),
             pltpu.VMEM((2, CHUNKS, w_rows, wide), bf16),
-            dma((3 + 4 * CHUNKS,)), dma((3, 8)), dma((3, 8)), dma((2, CHUNKS)), dma((2, CHUNKS)),
-            dma((2, 2, CHUNKS, n_fo, 2)), dma((2, CHUNKS, n_fo, 2)),
+            dma((3 + 4 * CHUNKS,)), dma((2, 8)), dma((3, 8)), dma((2, CHUNKS)), dma((2, CHUNKS)),
+            dma((2, n_fo + 1, 2)), dma((2, CHUNKS, n_fo, 2)),
             dma((2, 4)), dma((2, 4)), dma((2, 6)), dma((2, 6)),
-            dma((2, 2, CHUNKS, n_fo, 2)), dma((2, 2, CHUNKS, n_fo, 2)),
+            dma((2, n_fo, 2)), dma((2, CHUNKS, n_fo + 1, 2)),
             dma((2, CHUNKS)), dma((2, CHUNKS)),
         ],
         compiler_params=pltpu.CompilerParams(
@@ -545,10 +564,34 @@
     )(*(pltpu.with_memory_space_constraint(a, pltpu.HBM) for a in (*tokens, *weights)))
 
 
+def finish_kernel(*refs):
+    found, sums, results, (total, sems) = refs[0:4], refs[4:6], refs[6:10], refs[10:]
+    copies = [pltpu.make_async_copy(found[a], results[a], sems.at[a]) for a in range(2)]
+    for copy in copies:
+        copy.start()
+    for w in range(2):
+        total[w] = sums[w][...] + found[2 + w][...]
+        copies.append(pltpu.make_async_copy(total.at[w], results[2 + w], sems.at[2 + w]))
+        copies[-1].start()
+    for copy in copies:
+        copy.wait()
+
+
+def finish(found, sums):
+    return pl.pallas_call(
+        finish_kernel,
+        out_shape=[jax.ShapeDtypeStruct(a.shape, a.dtype) for a in found],
+        in_specs=[VMEM] * 6,
+        out_specs=[pl.BlockSpec(memory_space=pl.ANY)] * 4,
+        scratch_shapes=[pltpu.VMEM((2, *sums[0].shape), jnp.float32), pltpu.SemaphoreType.DMA((4,))],
+        compiler_params=pltpu.CompilerParams(vmem_limit_bytes=8_000_000),
+        name="finish",
+    )(*found, *sums)
+
+
 def on_device(n_fo, n_tp, x_late, x_early, cotangent, up_weight, down_weight, up_grad_sum, down_grad_sum):
-    output, input_grad, up_grad, down_grad = layer(
-        n_fo, n_tp, (x_early, cotangent, x_late), (up_weight, down_weight))
-    return (output, input_grad, up_grad_sum + up_grad, down_grad_sum + down_grad)
+    found = layer(n_fo, n_tp, (x_early, cotangent, x_late), (up_weight, down_weight))
+    return tuple(finish(found, (up_grad_sum, down_grad_sum)))
 
 
 def solution(mesh):

time: 125 us -> 118 us (0.944)
  Pallas kernels: 120 us -> 117 us
  other arithmetic: 2.26 us -> 0 us
  local copies, waits for them, and re-layouts: 1.82 us -> 0.01 us
    pallas_call x1, Pallas kernels: 120 us -> 116 us  [layer(): pl.pallas_call(functools.partial(layer_kernel, n_fo, n_tp), out_shape=[ja...]
    add x2 -> x0, other arithmetic: 2.26 us -> none  [the longest x1 1.15 us: on_device(): up_grad_sum + up_grad]
    unnamed x6 -> x4, local copies, waits for them, and re-layouts: 1.82 us -> 0.01 us
    pallas_call x0 -> x1, Pallas kernels: none -> 1.61 us  [finish(): pl.pallas_call(finish_kernel, out_shape=[jax.ShapeDtypeStruct(a.shape, a....]
where the time goes in v4:
time: 118 us
  Pallas kernels  117 us (99%)
    pallas_call x1, Pallas kernels, layer(): pl.pallas_call(functools.partial(layer_kernel, n_fo, n_tp), out_shape=[ja...  116 us

profile of v4, /device:TPU:0, one launch (start us, length us, event | category | flops | bytes accessed | tf_op | source)
XLA Modules:
  0.0 118.1 jit_solution(4675393621450958122)
XLA Ops:
  0.6 0.0 copy-start.1
  0.6 0.0 copy-start
  0.7 115.7 %layer.1 = (bf16[96,2048]{1,0:T(8,128)(2,1)S(1)}, bf16[96,2048]{1,0:T(8,128)(2,1)S(1)}, f32[256,1024]{1,0:T(8,128)S(1)}, f32[256,1024]{1,0:T(8,128)S(1)}) custom-call(bf16[96,2048]{1,0:T(8,128)(2,1)} %refs_0_.1, bf16[96,2048]{1,0:T(8,128)(2,1)} %refs_1_.1, bf16[96,2048]{1,0:T(8,128)(2,1)} %refs_2_.1, bf16[256,1024]{1,0:T(8,128)(2,1)} %refs_3_.1, ...), custom_call_target="tpu_custom_call" | custom-call | tf_op jit(solution)/shard_map/layer/pallas_call | solution.py:535
  116.3 0.0 copy-done.1
  116.3 0.0 copy-done
  116.3 1.6 %finish.1 = (bf16[96,2048]{1,0:T(8,128)(2,1)}, bf16[96,2048]{1,0:T(8,128)(2,1)}, f32[256,1024]{1,0:T(8,128)}, f32[256,1024]{1,0:T(8,128)}) custom-call(bf16[96,2048]{1,0:T(8,128)(2,1)S(1)} %get-tuple-element.8.refs_0_, bf16[96,2048]{1,0:T(8,128)(2,1)S(1)} %get-tuple-element.9.refs_1_, f32[256,1024]{1,0:T(8,128)S(1)} %get-tuple-element.10.refs_2_, ...), custom_call_target="tpu_custom_call" | custom-call | tf_op jit(solution)/shard_map/finish/pallas_call | solution.py:581
Async XLA Ops:
  0.6 115.7 %copy-start.1 = (f32[256,1024]{1,0:T(8,128)S(1)}, f32[256,1024]{1,0:T(8,128)}, u32[]{:S(2)}) copy-start(f32[256,1024]{1,0:T(8,128)} %refs_5_.1) | copy-start | bytes 3145732
  0.6 115.7 %copy-start = (f32[256,1024]{1,0:T(8,128)S(1)}, f32[256,1024]{1,0:T(8,128)}, u32[]{:S(2)}) copy-start(f32[256,1024]{1,0:T(8,128)} %refs_4_.3) | copy-start | bytes 3145732

commit v5 on v4

--- a/solution.py
+++ b/solution.py
@@ -54,8 +54,12 @@
     def side(part):
         return 1 - fi if part else fi
 
+    n_half = n_fo // 2
+    nearer = (fo >= n_half).astype(jnp.int32)
+    ends = first | last
+
     def open_way(way):
-        return jnp.logical_not(last) if way == 0 else jnp.logical_not(first)
+        return ((way == 0) & (fo < n_fo - 1)) | ((way == 1) & (fo > 0))
 
     def ahead(way):
         return (fo + 1 - 2 * way) * 2 + fi
@@ -138,7 +142,7 @@
 
     def along(w, c, source, part, way):
         dst = wts.at[w, c, source, side(part)]
-        sem = jnp.where(source == fo, n_fo, source) if way else source
+        sem = jnp.where((source == fo) & (way == 1), n_fo, source)
         return remote(dst, dst, zg_send.at[w, sem, part], zg_recv.at[w, c, source, part], ahead(way), tp)
 
     def send_along(w, c, source, part, way):
@@ -162,11 +166,11 @@
                 send_along(w, c, fo, 1, way)
 
     def incoming(way, distance):
-        source = fo - distance if way == 0 else fo + distance
+        source = fo - distance + 2 * distance * way
         return source, (source >= 0) & (source < n_fo)
 
     def forward(w, c, part, distance):
-        for way in range(2):
+        for way in (nearer, 1 - nearer):
             source, inside = incoming(way, distance)
 
             @pl.when(inside & open_way(way))
@@ -207,7 +211,6 @@
         relu = jnp.maximum(dot(flat(LATE), weight(UP, c), 1, 0), 0.0)
         hid[2, c] = (relu * relu).astype(jnp.bfloat16)
 
-    n_half = n_fo // 2
     d_half = width // 2
 
     def weight_grad(w, c, step):
@@ -246,7 +249,7 @@
     def grad(w, c, block, part, way, src=None, taker=None):
         held = g_in.at[way, w, c, block, part]
         taker = fo - 1 if taker is None else taker
-        sem = jnp.where(block == taker, n_fo, block) if way else block
+        sem = jnp.where((block == taker) & (way == 1), n_fo, block)
         return remote(held if src is None else src, held, zr_send.at[w, block, part],
                       zr_recv.at[w, c, sem, part], ahead(way), tp)
 
@@ -257,14 +260,15 @@
 
     def carry(c, start, stop):
         def position(q, carried):
-            for way in range(2):
-                hop = fo if way == 0 else n_fo - 1 - fo
+            for way in (nearer, 1 - nearer):
+                hop = jnp.where(way == 0, fo, n_fo - 1 - fo)
                 item = q - SKEW * (hop - 1)
                 w = 1 - item // (2 * n_fo)
-                block = farthest(way, item % (2 * n_fo) // 2)
+                k = item % (2 * n_fo) // 2
+                block = jnp.where(way == 0, n_fo - 1 - k, k)
                 part = 1 - item % 2
                 inside = (hop > 0) & (hop < n_fo - 1) & (item >= 0) & (item < 4 * n_fo)
-                beyond = fo < block if way == 0 else fo > block
+                beyond = jnp.where(way == 0, block - fo, fo - block) > 0
 
                 @pl.when(inside & beyond)
                 def _():
@@ -439,41 +443,51 @@
     forward(DOWN, 1, 1, 1)
     carry(0, 0, 2)
     forward_far(DOWN, 1, 0)
-    carry(0, 2, 3)
-    forward_far(DOWN, 1, 1)
     diagonal(LATE)
-    carry(0, 3, n_fo)
     from_sibling(LATE)
     activate_late(0)
+    forward_far(DOWN, 1, 1)
     token_begin(0, 2, DOWN)
-    carry(0, n_fo, 2 * n_fo + 2)
+    carry(0, 2, 3)
     token_begin(1, 1, UP)
+    carry(0, 3, n_fo)
     settle(UP, 1)
     activate(1)
-    carry(0, 2 * n_fo + 2, 2 * n_fo + 3)
-    weight_grad(DOWN, 1, 0)
-    weight_grad(DOWN, 1, 1)
-    carry(0, 2 * n_fo + 3, 4 * n_fo + SKEW * (n_fo - 3))
+
+    @pl.when(ends)
+    def _():
+        weight_grad(DOWN, 1, 0)
+        weight_grad(DOWN, 1, 1)
+
+    carry(0, n_fo, 2 * n_fo + 2)
     activate_late(1)
     settle(DOWN, 1)
     token_partial(0, 2, DOWN)
     spread(0, 3)
     hidden_grad(1)
+    carry(0, 2 * n_fo + 2, 2 * n_fo + 3)
     spread(0, 1)
-    carry(1, 0, 1)
     owned(DOWN, 0, 1)
     token_partial(1, 1, UP)
+
+    @pl.when(jnp.logical_not(ends))
+    def _():
+        weight_grad(DOWN, 1, 0)
+        weight_grad(DOWN, 1, 1)
+
+    carry(0, 2 * n_fo + 3, 4 * n_fo + SKEW * (n_fo - 3))
     spread(1, 3)
-    carry(1, 1, 2)
+    carry(1, 0, 1)
     spread(1, 1)
     spread(0, 2)
+    carry(1, 1, 2)
     weight_grad(UP, 1, 0)
-    carry(1, 2, 3)
     spread(1, 2)
     weight_grad(UP, 1, 1)
     owned(UP, 0, 1)
+    relay(0)
+    carry(1, 2, 3)
     carry(1, 3, n_fo)
-    relay(0)
     carry(1, n_fo, 2 * n_fo)
     for w in (DOWN, UP):
         owned(w, 0, 0)

time: 118 us -> 115 us (0.975)
  Pallas kernels: 117 us -> 114 us
    pallas_call x1, Pallas kernels: 116 us -> 113 us  [layer(): pl.pallas_call(functools.partial(layer_kernel, n_fo, n_tp), out_shape=[ja...]
where the time goes in v5:
time: 115 us
  Pallas kernels  114 us (99%)
    pallas_call x1, Pallas kernels, layer(): pl.pallas_call(functools.partial(layer_kernel, n_fo, n_tp), out_shape=[ja...  113 us

profile of v5, /device:TPU:0, one launch (start us, length us, event | category | flops | bytes accessed | tf_op | source)
XLA Modules:
  0.0 115.3 jit_solution(14161679244386325216)
XLA Ops:
  0.6 0.0 copy-start.1
  0.6 0.0 copy-start
  0.7 112.9 %layer.1 = (bf16[96,2048]{1,0:T(8,128)(2,1)S(1)}, bf16[96,2048]{1,0:T(8,128)(2,1)S(1)}, f32[256,1024]{1,0:T(8,128)S(1)}, f32[256,1024]{1,0:T(8,128)S(1)}) custom-call(bf16[96,2048]{1,0:T(8,128)(2,1)} %refs_0_.1, bf16[96,2048]{1,0:T(8,128)(2,1)} %refs_1_.1, bf16[96,2048]{1,0:T(8,128)(2,1)} %refs_2_.1, bf16[256,1024]{1,0:T(8,128)(2,1)} %refs_3_.1, ...), custom_call_target="tpu_custom_call" | custom-call | tf_op jit(solution)/shard_map/layer/pallas_call | solution.py:549
  113.5 0.0 copy-done.1
  113.5 0.0 copy-done
  113.5 1.6 %finish.1 = (bf16[96,2048]{1,0:T(8,128)(2,1)}, bf16[96,2048]{1,0:T(8,128)(2,1)}, f32[256,1024]{1,0:T(8,128)}, f32[256,1024]{1,0:T(8,128)}) custom-call(bf16[96,2048]{1,0:T(8,128)(2,1)S(1)} %get-tuple-element.8.refs_0_, bf16[96,2048]{1,0:T(8,128)(2,1)S(1)} %get-tuple-element.9.refs_1_, f32[256,1024]{1,0:T(8,128)S(1)} %get-tuple-element.10.refs_2_, ...), custom_call_target="tpu_custom_call" | custom-call | tf_op jit(solution)/shard_map/finish/pallas_call | solution.py:595
Async XLA Ops:
  0.6 112.9 %copy-start.1 = (f32[256,1024]{1,0:T(8,128)S(1)}, f32[256,1024]{1,0:T(8,128)}, u32[]{:S(2)}) copy-start(f32[256,1024]{1,0:T(8,128)} %refs_5_.1) | copy-start | bytes 3145732
  0.6 112.9 %copy-start = (f32[256,1024]{1,0:T(8,128)S(1)}, f32[256,1024]{1,0:T(8,128)}, u32[]{:S(2)}) copy-start(f32[256,1024]{1,0:T(8,128)} %refs_4_.3) | copy-start | bytes 3145732
